TPU v7x, 32 devices: a whole 2x2x4 slice. The times are simulated.
32 devices in a mesh: grp: 2 (over y), sp: 4 (over z), tp: 4 (over x, core).
Axes of the slice: x: 2, y: 2, z: 4, core: 2. Of those that a mesh axis runs over, the one named last changes fastest.
Arguments:
- inputs: bfloat16 [2048, 2048], P(('grp', 'sp'), 'tp'), parts along dimension 0, may hold values from -20 to 20
- norm_gain: bfloat16 [2048], replicated, may hold values from 0.099609375 to 1.8984375
- w_conv_in: bfloat16 [1024, 2048], P('tp'), may hold values from -0.125 to 0.125
- w_conv_gate: bfloat16 [1024, 2048], P('tp'), may hold values from -0.125 to 0.125
- conv_kernel: bfloat16 [31, 1024], P(None, 'tp'), may hold values from -4.3105272 to 4.3105272
- ln_gain: bfloat16 [1024], P('tp'), may hold values from 0.099609375 to 1.8984375
- w_query: bfloat16 [1024, 2048], P('tp'), may hold values from -0.53033009 to 0.53033009
- w_key: bfloat16 [1024, 2048], P('tp'), may hold values from -0.53033009 to 0.53033009
- w_value: bfloat16 [1024, 2048], P('tp'), may hold values from -0.125 to 0.125
- cum_gate: float32 [16, 2048], P('tp', ('grp', 'sp')), parts along dimension 1, may hold values from -1024 to 0, as said below
- w_conv_out: bfloat16 [1024, 2048], P('tp'), may hold values from -0.125 to 0.125
- w_attn_out: bfloat16 [1024, 2048], P('tp'), may hold values from -0.125 to 0.125
Outputs:
- mixed: bfloat16 [2048, 2048], P(('grp', 'sp', 'tp')), parts along dimension 0
- log_total: float32 [16, 2048], P('tp', ('grp', 'sp')), parts along dimension 1
There are 2 independent parts, one for each index of `grp`. A program takes and returns all parts, laid end to end along the dimension named above; an argument that names none is the same for every part. Nothing has to cross between parts.
Inputs may be any that keep to these rules, and one draw needn't show every extreme that they name: cum_gate never rises along positions: entry t is the sum of the head's log forget gates at positions 0 to t.
All inputs are finite; a program needn't handle non-finite values.
Results may differ from a plain program's by a relative error of at most 0.0144.
Values may be sent and summed in bfloat16 or wider, within the bound.
A program may use at most 64 MiB of HBM per device.

v0:
```python
import jax
import jax.numpy as jnp
from jax import lax
from jax.sharding import PartitionSpec as P

D = 2048
CONV_CH = 1024


neg_large = -1e30


def passed_along(block, axis, distance):
    devices = range(lax.axis_size(axis))
    route = [(i - distance, i) for i in devices if i - distance in devices]
    return lax.ppermute(block, axis, route)


def block_terms(q_blk, q_cum, k_blk, v_blk, k_cum, q_first, k_first):
    score_scale = q_blk.shape[2] ** (-0.5)
    scores = (
        jnp.einsum("qhd,khd->hqk", q_blk, k_blk, preferred_element_type=jnp.float32) * score_scale
    )
    scores = scores + q_cum[:, :, None] - k_cum[:, None, :]
    q_pos = q_first + jnp.arange(q_blk.shape[0], dtype=jnp.int32)
    k_pos = k_first + jnp.arange(k_blk.shape[0], dtype=jnp.int32)
    allowed = k_pos[None, :] <= q_pos[:, None]
    scores = jnp.where(allowed[None], scores, -jnp.inf)
    block_top = jnp.max(scores, axis=-1)
    weights = jnp.exp(scores - block_top[..., None])
    block_total = jnp.sum(weights, axis=-1)
    block_out = jnp.einsum(
        "hqk,khd->hqd", weights.astype(jnp.bfloat16), v_blk, preferred_element_type=jnp.float32
    ).astype(jnp.bfloat16)
    return (block_top, block_total, block_out)


def merge_terms(state, terms):
    top_now, total_now, acc_now = state
    block_top, block_total, block_out = terms
    top_new = jnp.maximum(top_now, block_top)
    keep_old = jnp.exp(top_now - top_new)
    keep_new = jnp.exp(block_top - top_new)
    return (
        top_new,
        total_now * keep_old + block_total * keep_new,
        acc_now * keep_old[..., None] + block_out.astype(jnp.float32) * keep_new[..., None],
    )


def local(
    inputs,
    norm_gain,
    w_conv_in,
    w_conv_gate,
    conv_kernel,
    ln_gain,
    w_query,
    w_key,
    w_value,
    cum_gate,
    w_conv_out,
    w_attn_out,
):
    rows_here = inputs.shape[0]
    conv_width = w_conv_in.shape[0]
    attn_width = w_query.shape[0]
    heads_here = cum_gate.shape[0]
    head_dim = attn_width // heads_here
    taps_count = conv_kernel.shape[0]
    w_all = jnp.concatenate([w_conv_in, w_conv_gate, w_query, w_key, w_value], axis=0)
    gain_all = norm_gain.astype(jnp.float32)
    contract_dims = (((1,), (1,)), ((), ()))
    piece_f = lax.all_gather(inputs, "tp", axis=1, tiled=True).astype(jnp.float32)
    scaled_piece = (piece_f * gain_all[None, :]).astype(jnp.bfloat16)
    raw_proj = lax.dot_general(
        scaled_piece, w_all, contract_dims, preferred_element_type=jnp.float32
    )
    squares = jnp.sum(piece_f * piece_f, axis=1)
    rms = lax.rsqrt(squares / D + 1e-06)[:, None]
    proj = raw_proj * rms
    conv_in = proj[:, :conv_width]
    conv_gate = proj[:, conv_width : 2 * conv_width]
    query = proj[:, 2 * conv_width : 2 * conv_width + attn_width].astype(jnp.bfloat16)
    key_rows = proj[:, 2 * conv_width + attn_width : 2 * conv_width + 2 * attn_width].astype(
        jnp.bfloat16
    )
    value = proj[:, 2 * conv_width + 2 * attn_width :].astype(jnp.bfloat16)
    glu = (conv_in * jax.nn.sigmoid(conv_gate)).astype(jnp.bfloat16)
    rim_rows = passed_along(glu[rows_here - (taps_count - 1) :], "sp", 1)
    extended = jnp.concatenate([rim_rows, glu], axis=0)
    kernel = conv_kernel.astype(jnp.float32)
    conv_sum = jnp.zeros((rows_here, conv_width), jnp.float32)
    for tap_idx in range(taps_count):
        conv_sum = (
            conv_sum
            + extended[tap_idx : tap_idx + rows_here].astype(jnp.float32) * kernel[tap_idx][None, :]
        )
    chan_first, chan_second = lax.psum(
        (jnp.sum(conv_sum, axis=1), jnp.sum(conv_sum * conv_sum, axis=1)), "tp"
    )
    chan_mean = (chan_first / CONV_CH)[:, None]
    chan_var = (chan_second / CONV_CH)[:, None] - chan_mean * chan_mean
    normed = (
        (conv_sum - chan_mean) * lax.rsqrt(chan_var + 1e-05) * ln_gain.astype(jnp.float32)[None, :]
    )
    conv_out = jax.nn.silu(normed).astype(jnp.bfloat16)
    q_heads = query.reshape(rows_here, heads_here, head_dim)
    cum_all = lax.all_gather(cum_gate.T, "sp", axis=0, tiled=True)
    own_first = lax.axis_index("sp") * rows_here
    start_state = (
        jnp.full((heads_here, rows_here), neg_large, jnp.float32),
        jnp.zeros((heads_here, rows_here), jnp.float32),
        jnp.zeros((heads_here, rows_here, head_dim), jnp.float32),
    )
    state = start_state
    k_piece = lax.all_gather(key_rows, "sp", axis=0, tiled=True)
    v_piece = lax.all_gather(value, "sp", axis=0, tiled=True)
    block_count = k_piece.shape[0] // rows_here
    k_split = k_piece.reshape(block_count, rows_here, heads_here, head_dim)
    v_split = v_piece.reshape(block_count, rows_here, heads_here, head_dim)

    def visit(carry, item):
        k_blk, v_blk, block_idx = item
        k_first = block_idx * rows_here
        k_cum = lax.dynamic_slice_in_dim(cum_all, k_first, rows_here, 0).T

        def take_block(inner):
            return merge_terms(
                inner, block_terms(q_heads, cum_gate, k_blk, v_blk, k_cum, own_first, k_first)
            )

        def skip_block(inner):
            return inner

        return (lax.cond(k_first <= own_first, take_block, skip_block, carry), None)

    state, unused = lax.scan(
        visit, state, (k_split, v_split, jnp.arange(block_count, dtype=jnp.int32))
    )
    top_all, total_all, acc_all = state
    attn_out = (
        (acc_all / total_all[..., None])
        .transpose(1, 0, 2)
        .reshape(rows_here, attn_width)
        .astype(jnp.bfloat16)
    )
    log_total = top_all + jnp.log(total_all)
    mixed = lax.psum_scatter(
        (
            jnp.dot(conv_out, w_conv_out, preferred_element_type=jnp.float32)
            + jnp.dot(attn_out, w_attn_out, preferred_element_type=jnp.float32)
        ).astype(jnp.bfloat16),
        "tp",
        scatter_dimension=0,
        tiled=True,
    )
    return (mixed, log_total)


def solution(mesh):
    in_specs = (
        P(("grp", "sp"), "tp"),
        P(),
        P("tp", None),
        P("tp", None),
        P(None, "tp"),
        P("tp"),
        P("tp", None),
        P("tp", None),
        P("tp", None),
        P("tp", ("grp", "sp")),
        P("tp", None),
        P("tp", None),
    )
    out_specs = (P(("grp", "sp", "tp"), None), P("tp", ("grp", "sp")))
    return jax.shard_map(local, mesh=mesh, in_specs=in_specs, out_specs=out_specs, check_vma=False)
```

profile of v0, /device:TPU:0, one launch (start us, length us, event | category | flops | bytes accessed | tf_op | source)
XLA Modules:
  0.0 143.7 jit_solution(8039466235319042645)
XLA Ops:
  7.2 0.7 all-gather.2.cloned.1.call-update
  8.0 1.6 %fusion.66 = (f32[1,256]{1,0:T(1,128)S(1)}, f32[1,256]{1,0:T(1,128)}, f32[1,256]{1,0:T(1,128)}, f32[1,256]{1,0:T(1,128)}, f32[1,256]{1,0:T(1,128)}, /*index=5*/f...) fusion(bf16[31,256]{1,0:T(8,128)(2,1)} %param.20), kind=kLoop, calls=%fused_computation.130 | loop fusion | bytes 24576 | tf_op jit(solution)/shard_map/slice | solution.py:97
  9.6 0.7 convert_element_type.148
  10.3 1.2 convert_element_type.183
  11.5 16.6 %all_gather.13 = f32[1024,4]{0,1:T(4,128)} all-gather(f32[256,4]{0,1:T(4,128)} %bitcast.93), channel_id=1, replica_groups=mesh['grp'=2,'sp'=4,'tp'=4] {'sp'}, dimensions={0}, use_global_device_ids=true | all-gather | bytes 20480 | tf_op jit(solution)/shard_map/all_gather | solution.py:109
  28.0 1.7 %fusion.65 = (f32[1,256]{1,0:T(1,128)}, f32[1,256]{1,0:T(1,128)}, f32[1,256]{1,0:T(1,128)}, f32[1,256]{1,0:T(1,128)}, f32[1,256]{1,0:T(1,128)}, /*index=5*/f32[1...) fusion(bf16[31,256]{1,0:T(8,128)(2,1)} %param.20), kind=kLoop, calls=%fused_computation.129 | loop fusion | bytes 38912 | tf_op jit(solution)/shard_map/slice | solution.py:97
  29.7 2.3 %constant_dynamic-update-slice_fusion.4 = bf16[1280,2048]{1,0:T(8,128)(2,1)} fusion(bf16[256,2048]{1,0:T(8,128)(2,1)} %param.18), kind=kLoop, calls=%fused_computation.120 | loop fusion | bytes 2097152
  32.0 2.4 %constant_dynamic-update-slice_fusion.3 = bf16[1280,2048]{1,0:T(8,128)(2,1)} fusion(bf16[1280,2048]{1,0:T(8,128)(2,1)} %constant_dynamic-update-slice_fusion.4, bf16[256,2048]{1,0:T(8,128)(2,1)} %param.19), kind=kLoop, calls=%fused_computation.119 | loop fusion | bytes 2097152
  34.4 1.1 constant_dynamic-update-slice_fusion.2
  35.4 1.0 constant_dynamic-update-slice_fusion.1
  36.5 1.0 constant_dynamic-update-slice_fusion
  37.5 1.5 %fusion.19 = f32[256]{0:T(256)S(1)} fusion(bf16[256,2048]{1,0:T(8,128)(2,1)} %all-gather.2.cloned.1.call-done), kind=kLoop, calls=%fused_computation.32 | loop fusion | flops 1572608 | bytes 1049600 | tf_op jit(solution)/shard_map/reduce_sum | solution.py:79
  39.0 4.4 %fusion.67 = (bf16[256,1280]{1,0:T(8,128)(2,1)S(1)}, f32[256,1280]{1,0:T(8,128)S(1)}) fusion(f32[256]{0:T(256)S(1)} %add_rsqrt_fusion.1, bf16[1280,2048]{1,0:T(8,128)(2,1)} %constant_dynamic-update-slice_fusion, bf16[256,2048]{1,0:T(8,128)(2,1)} %all-gather.2.cloned.1.call-done, f32[2048]{0:T(1024)S(1)} %convert_element_type.148), kind=kOutput, calls=%fused_computation.131 | convolution fusion | flops 1344405504 | bytes 8266752 | tf_op jit(solution)/shard_map/dot_general | solution.py:76
  44.1 3.3 %collective-permute-start = (bf16[30,256]{1,0:T(8,128)(2,1)}, bf16[30,256]{1,0:T(8,128)(2,1)}, u32[]{:S(2)}, u32[]{:S(2)}) collective-permute-start(bf16[30,256]{1,0:T(8,128)(2,1)} %slice.273), channel_id=1, source_target_pairs={{0,4},{4,8},{8,12},{1,5},{5,9},{9,13},{2,6},{6,10},{10,14},{3,7},{... | collective-permute-start | bytes 46088 | tf_op jit(solution)/shard_map/ppermute | solution.py:16
  48.1 14.8 %all_gather.14 = bf16[1024,256]{1,0:T(8,128)(2,1)S(1)} all-gather(bf16[256,256]{1,0:T(8,128)(2,1)S(1)} %get-tuple-element.220), channel_id=1, replica_groups=mesh['grp'=2,'sp'=4,'tp'=4] {'sp'}, dimensions={0}, use_global_device_ids=true | all-gather | bytes 655360 | tf_op jit(solution)/shard_map/all_gather | solution.py:117
  63.9 1.7 %copy.20 = bf16[256,256]{0,1:T(8,128)(2,1)} copy(bf16[256,256]{1,0:T(8,128)(2,1)} %get-tuple-element.219) | data formatting | bytes 262144 | tf_op jit(solution)/shard_map/slice | solution.py:84
  65.5 14.9 %all_gather.15 = bf16[1024,256]{1,0:T(8,128)(2,1)S(1)} all-gather(bf16[256,256]{1,0:T(8,128)(2,1)S(1)} %get-tuple-element.218), channel_id=1, replica_groups=mesh['grp'=2,'sp'=4,'tp'=4] {'sp'}, dimensions={0}, use_global_device_ids=true | all-gather | bytes 655360 | tf_op jit(solution)/shard_map/all_gather | solution.py:118
  81.9 11.9 %while.14 = (s32[]{:T(128)}, f32[4,256]{1,0:T(4,128)S(1)}, f32[4,256]{1,0:T(4,128)S(1)}, f32[4,256,64]{1,2,0:T(8,128)S(1)}, s32[4]{0:T(128)}, /*index=5*/s32[]{:...) while((s32[]{:T(128)}, f32[4,256]{1,0:T(4,128)S(1)}, ...), condition=%wide.region_10.11_spmd, body=%wide.region_5.10_spmd.sunk | while | flops 69865992 | bytes 4272513 | solution.py:138
  82.0 1.3 dynamic_slice.38
  83.8 0.7 dynamic-slice_bitcast_fusion.2
  84.5 2.0 %conditional.2 = ((f32[4,256]{1,0:T(4,128)S(1)}, f32[4,256]{1,0:T(4,128)S(1)}, f32[4,256,64]{1,2,0:T(8,128)S(1)})) conditional(s32[]{:T(128)} %convert_element_type.284, (f32[4,256]{1,0:T(4,128)S(1)}, f32[4,256]{1,0:T(4,128)S(1)}, f32[4,256,64]{1,2,0:T(8,128)S(1)}) %tuple.77, (s32[]{:T(128)}, s32[]{:T(128)}, bf16[4,256,4,64]{1,3,2,0:T(8,128)(2,1)S(1)}, ...), branch_computations={%region_6.6_spmd, %region_7.9_spmd} | conditional | flops 69865984 | bytes 4263984 | solution.py:136
  84.6 1.4 fusion.63
  86.5 1.2 dynamic_slice.38
  88.3 0.7 dynamic-slice_bitcast_fusion.2
  89.0 1.2 dynamic_slice.38
  90.7 0.7 dynamic-slice_bitcast_fusion.2
  91.4 1.2 dynamic_slice.38
  93.9 3.1 %fusion.62 = (f32[256]{0:T(256)S(1)}, f32[256]{0:T(256)S(1)}, f32[256,256]{1,0:T(8,128)S(1)}) fusion(f32[256]{0:T(256)} %bitcast.73, bf16[256,256]{1,0:T(8,128)(2,1)S(1)} %fusion.26, f32[256]{0:T(256)} %bitcast.72, bf16[30,256]{1,0:T(8,128)(2,1)} %collective-permute-done, f32[256]{0:T(256)} %bitcast.71, f32[256]{0:T(256)} %bitcast.70, f32[256]{0:T(256)} %bitcast.69, ...), kind=kLoop, calls=%fused_computation.126 | loop fusion | flops 12123648 | bytes 442368 | tf_op jit(solution)/shard_map/reduce_sum | solution.py:100
  97.0 5.7 %all-reduce = (f32[256]{0:T(256)S(1)}, f32[256]{0:T(256)S(1)}) all-reduce(f32[256]{0:T(256)S(1)} %get-tuple-element.184, f32[256]{0:T(256)S(1)} %get-tuple-element.183), channel_id=1, replica_groups=mesh['grp'=2,'sp'=4,'tp'=4] {'tp'}, use_global_device_ids=true, to_apply=%region_4.0 | all-reduce | flops 512 | bytes 4096 | tf_op jit(solution)/shard_map/psum | solution.py:99
  102.7 1.1 fusion.27
  103.8 1.4 %fusion.17 = bf16[256,2048]{1,0:T(8,128)(2,1)} fusion(f32[256,2048]{1,0:T(8,128)S(1)} %fusion.27, bf16[256,256]{0,1:T(8,128)(2,1)S(1)} %bitcast.60, bf16[256,2048]{1,0:T(8,128)(2,1)S(1)} %copy-done.4), kind=kOutput, calls=%fused_computation.30 | convolution fusion | flops 269484032 | bytes 4325376 | tf_op jit(solution)/shard_map/dot_general | solution.py:152
  105.9 30.9 %reduce-scatter.2.cloned.1.call-done = bf16[64,2048]{1,0:T(8,128)(2,1)} async-done(((bf16[256,2048]{1,0:T(8,128)(2,1)}), bf16[64,2048]{1,0:T(8,128)(2,1)}) %reduce-scatter.2.cloned.1.call-update) | async-done | bytes 262160 | tf_op jit(solution)/shard_map/reduce_scatter | solution.py:149
  (39 shorter events, 5.8 us)
Async XLA Ops:
  7.2 95.5 %copy-start = (bf16[256,2048]{1,0:T(8,128)(2,1)S(1)}, bf16[256,2048]{1,0:T(8,128)(2,1)}, u32[]{:S(2)}) copy-start(bf16[256,2048]{1,0:T(8,128)(2,1)} %param.26) | copy-start | bytes 3145732
  7.2 27.2 %copy-start.1 = (bf16[256,2048]{1,0:T(8,128)(2,1)S(1)}, bf16[256,2048]{1,0:T(8,128)(2,1)}, u32[]{:S(2)}) copy-start(bf16[256,2048]{1,0:T(8,128)(2,1)} %param.22) | copy-start | bytes 3145732
  7.2 28.2 %copy-start.2 = (bf16[256,2048]{1,0:T(8,128)(2,1)S(1)}, bf16[256,2048]{1,0:T(8,128)(2,1)}, u32[]{:S(2)}) copy-start(bf16[256,2048]{1,0:T(8,128)(2,1)} %param.23) | copy-start | bytes 3145732
  7.2 30.3 %all-gather.2.cloned.1.call-start = ((), (), s32[]{:S(2)}) async-start(), calls=%async_computation.1 | async-start | bytes 1310720 | tf_op jit(solution)/shard_map/all_gather | solution.py:74
  7.9 128.9 %reduce-scatter.2.cloned.1.call-start = ((), (), s32[]{:S(2)}) async-start(), calls=%async_computation.2 | async-start | bytes 1310720 | tf_op jit(solution)/shard_map/reduce_scatter | solution.py:149
  11.5 25.0 %copy-start.3 = (bf16[256,2048]{1,0:T(8,128)(2,1)S(1)}, bf16[256,2048]{1,0:T(8,128)(2,1)}, u32[]{:S(2)}) copy-start(bf16[256,2048]{1,0:T(8,128)(2,1)} %param.24) | copy-start | bytes 3145732
  44.1 49.8 %collective-permute-start = (bf16[30,256]{1,0:T(8,128)(2,1)}, bf16[30,256]{1,0:T(8,128)(2,1)}, u32[]{:S(2)}, u32[]{:S(2)}) collective-permute-start(bf16[30,256]{1,0:T(8,128)(2,1)} %slice.273), channel_id=1, source_target_pairs={{0,4},{4,8},{8,12},{1,5},{5,9},{9,13},{2,6},{6,10},{10,14},{3,7},{... | collective-permute-start | bytes 46088 | tf_op jit(solution)/shard_map/ppermute | solution.py:16
  81.9 21.9 %copy-start.4 = (bf16[256,2048]{1,0:T(8,128)(2,1)S(1)}, bf16[256,2048]{1,0:T(8,128)(2,1)}, u32[]{:S(2)}) copy-start(bf16[256,2048]{1,0:T(8,128)(2,1)} %param.27) | copy-start | bytes 3145732
Sparse Core Ops, SparseCore 0:
  9.6 19.4 all-gather.1
  105.4 31.3 reduce-scatter.1
where the time goes:
time: 144 us
  blocking collectives  51.9 us (36%)
  waiting for transfers between devices  31.6 us (22%)
  local copies, waits for them, and re-layouts  24.1 us (17%)
  between operations  14.2 us (10%)
  matrix products  8.65 us (6%)
  other arithmetic  7.49 us (5%)
  starting transfers between devices  3.4 us (2%)
  loops' own time  2.32 us (2%)
    reduce_scatter x1, waiting for transfers between devices, local(): lax.psum_scatter((jnp.dot(conv_out, w_conv_out, preferred_element_type=jn...  30.9 us
    all_gather x1, blocking collectives, local(): cum_all = lax.all_gather(cum_gate.T, 'sp', axis=0, tiled=True)  16.6 us
    all_gather x1, blocking collectives, local(): v_piece = lax.all_gather(value, 'sp', axis=0, tiled=True)  14.9 us
    all_gather x1, blocking collectives, local(): k_piece = lax.all_gather(key_rows, 'sp', axis=0, tiled=True)  14.8 us
    unnamed x14, local copies, waits for them, and re-layouts  6.79 us
    psum x1, blocking collectives, local(): lax.psum((jnp.sum(conv_sum, axis=1), jnp.sum(conv_sum * conv_sum, axis=1)...  5.67 us
    dynamic_slice x4, local copies, waits for them, and re-layouts, local(): lax.scan(visit, state, (k_split, v_split, jnp.arange(block_count, dtype=j...  4.92 us
    dot_general x1, matrix products, local(): lax.dot_general(scaled_piece, w_all, contract_dims, preferred_element_typ...  4.38 us
  transfers between devices with their start and end apart: 3, of which 1 were waited for; matrix products, arithmetic and copies ran while one was open for 19% of the time, Pallas kernels for 0%

commit v1 on v0

--- a/solution.py
+++ b/solution.py
@@ -1,10 +1,14 @@
+import functools
 import jax
 import jax.numpy as jnp
 from jax import lax
+from jax.experimental import pallas as pl
+from jax.experimental.pallas import tpu as pltpu
 from jax.sharding import PartitionSpec as P
 
 D = 2048
 CONV_CH = 1024
+HEADS = 16
 
 
 neg_large = -1e30
@@ -158,6 +162,557 @@
     return (mixed, log_total)
 
 
+AG_CHUNKS = 4
+OUT_CHUNKS = 4
+MESH = pl.DeviceIdType.MESH
+NT = (((1,), (1,)), ((), ()))
+
+
+def fused_kernel(
+    n_sp,
+    n_tp,
+    x_hbm,
+    gain_ref,
+    wci_hbm,
+    wcg_hbm,
+    ck_ref,
+    lng_ref,
+    wq_hbm,
+    wk_hbm,
+    wv_hbm,
+    cum_ref,
+    wco_hbm,
+    wao_hbm,
+    out_ref,
+    log_ref,
+    xg,
+    xs,
+    wbuf,
+    wco,
+    wao,
+    acc,
+    ss,
+    zsend,
+    zrecv,
+    q_s,
+    k_s,
+    v_s,
+    cum_recv,
+    ext,
+    glu_s,
+    halo,
+    csum,
+    st_send,
+    st_recv,
+    cpart,
+    ret_send,
+    ret_recv,
+    att_s,
+    lse_send,
+    lse_recv,
+    d_send,
+    d_recv,
+    x_send,
+    x_recv,
+    own_part,
+    wsem,
+    owsem,
+    xsem,
+    ag_send,
+    ag_recv,
+    zs_sem,
+    zr_sem,
+    cs_sem,
+    cr_sem,
+    hs_sem,
+    hr_sem,
+    ss_sem,
+    sr_sem,
+    rs_sem,
+    rr_sem,
+    ls_sem,
+    lr_sem,
+    ds_sem,
+    dr_sem,
+    xs_sem,
+    xr_sem,
+):
+    f32, bf16 = jnp.float32, jnp.bfloat16
+    z = lax.axis_index("sp")
+    me = lax.axis_index("tp")
+    chip, core = me // 2, me % 2
+    chips = n_tp // 2
+    rows, width = x_hbm.shape
+    conv_w = wci_hbm.shape[0]
+    attn_w = wq_hbm.shape[0]
+    heads = n_sp
+    hd = attn_w // heads
+    d_all = wci_hbm.shape[1]
+    partner = chip * 2 + 1 - core
+
+    def remote(src, dst, s, r, dev):
+        return pltpu.make_async_remote_copy(
+            src_ref=src, dst_ref=dst, send_sem=s, recv_sem=r, device_id=dev, device_id_type=MESH
+        )
+
+    def same_core(dist):
+        return lax.rem(chip + dist, chips) * 2 + core
+
+    def other_core(dist):
+        return lax.rem(chip + dist, chips) * 2 + 1 - core
+
+    def piece_owner(rel):
+        return same_core(rel // 2) if rel % 2 == 0 else other_core(rel // 2)
+
+    def piece_source(rel):
+        back = chips - rel // 2
+        return same_core(back) if rel % 2 == 0 else other_core(back)
+
+    barrier = pltpu.get_barrier_semaphore()
+    for rel in range(1, n_tp):
+        pl.semaphore_signal(
+            barrier, inc=1, device_id={"tp": piece_owner(rel)}, device_id_type=MESH
+        )
+    for dist in range(1, n_sp):
+        pl.semaphore_signal(
+            barrier, inc=1, device_id={"sp": lax.rem(z + dist, n_sp)}, device_id_type=MESH
+        )
+
+    own_copy = pltpu.make_async_copy(x_hbm, xg.at[0], xsem)
+    own_copy.start()
+    loads = []
+    for h in range(heads):
+        loads.append((wq_hbm.at[pl.ds(h * hd, hd)], wbuf.at[pl.ds(2 * h * hd, hd)]))
+        loads.append((wk_hbm.at[pl.ds(h * hd, hd)], wbuf.at[pl.ds((2 * h + 1) * hd, hd)]))
+    loads.append((wv_hbm, wbuf.at[pl.ds(2 * attn_w, attn_w)]))
+    qkv_loads = len(loads)
+    qkv_w = 3 * attn_w
+    loads.append((wci_hbm, wbuf.at[pl.ds(qkv_w, conv_w)]))
+    loads.append((wcg_hbm, wbuf.at[pl.ds(qkv_w + conv_w, conv_w)]))
+    wcopies = [pltpu.make_async_copy(a, b, wsem.at[i]) for i, (a, b) in enumerate(loads)]
+    wco_copy = pltpu.make_async_copy(wco_hbm, wco, owsem.at[0])
+    wao_copy = pltpu.make_async_copy(wao_hbm, wao, owsem.at[1])
+    for c in wcopies:
+        c.start()
+    wco_copy.start()
+    wao_copy.start()
+
+    pl.semaphore_wait(barrier, n_tp - 1 + n_sp - 1)
+
+    rc = rows // AG_CHUNKS
+
+    def ag_copy(rel, kind, c):
+        r = pl.ds(c * rc, rc)
+        if kind == "own":
+            return remote(
+                x_hbm.at[r], xg.at[rel, r], ag_send.at[rel, c], ag_recv.at[rel, c],
+                {"tp": piece_owner(rel)},
+            )
+        return remote(
+            xg.at[rel - 1, r], xg.at[rel, r], ag_send.at[rel, c], ag_recv.at[rel, c],
+            {"tp": partner},
+        )
+
+    ag = {}
+    for c in range(AG_CHUNKS):
+        for dist in range(1, chips):
+            ag[2 * dist, c] = ag_copy(2 * dist, "own", c)
+            ag[2 * dist, c].start()
+    for c in range(AG_CHUNKS):
+        ag[1, c] = ag_copy(1, "own", c)
+        ag[1, c].start()
+    cums = []
+    for dist in range(1, n_sp):
+        cp = remote(
+            cum_ref, cum_recv.at[z], cs_sem.at[dist], cr_sem.at[dist],
+            {"sp": lax.rem(z + dist, n_sp)},
+        )
+        cp.start()
+        cums.append(cp)
+    cum_recv[z] = cum_ref[...]
+
+    def prepare(rel, c0, n):
+        r = pl.ds(c0, n)
+        owner = piece_source(rel)
+        raw = xg[rel, r].astype(f32)
+        g = gain_ref[:, pl.ds(pl.multiple_of(owner * width, width), width)].astype(f32)
+        xs[rel, r] = (raw * g).astype(bf16)
+        return jnp.sum(raw * raw, axis=1, keepdims=True)
+
+    def wcols(rel, first, n):
+        owner = piece_source(rel)
+        return wbuf[pl.ds(first, n), pl.ds(pl.multiple_of(owner * width, width), width)]
+
+    own_copy.wait()
+    ss[...] = prepare(0, 0, rows)
+    for c in wcopies[:qkv_loads]:
+        c.wait()
+    acc[:, :qkv_w] = lax.dot_general(xs[0], wcols(0, 0, qkv_w), NT, preferred_element_type=f32)
+    for c in wcopies[qkv_loads:]:
+        c.wait()
+    acc[:, qkv_w:] = lax.dot_general(
+        xs[0], wcols(0, qkv_w, 2 * conv_w), NT, preferred_element_type=f32
+    )
+    for c in range(AG_CHUNKS):
+        ag[1, c].wait_recv()
+    ss[...] += prepare(1, 0, rows)
+    acc[...] += lax.dot_general(
+        xs[1], wcols(1, 0, qkv_w + 2 * conv_w), NT, preferred_element_type=f32
+    )
+
+    half = rc // 2
+    for c in range(AG_CHUNKS):
+        r = pl.ds(c * rc, rc)
+        for dist in range(1, chips):
+            ag[2 * dist, c].wait_recv()
+            ag[2 * dist + 1, c] = ag_copy(2 * dist + 1, "relay", c)
+            ag[2 * dist + 1, c].start()
+        total = acc[r, :qkv_w]
+        sq = ss[r]
+        for dist in range(1, chips):
+            for rel in (2 * dist, 2 * dist + 1):
+                if rel % 2 == 1:
+                    ag[rel, c].wait_recv()
+                sq = sq + prepare(rel, c * rc, rc)
+                total = total + lax.dot_general(
+                    xs[rel, r], wcols(rel, 0, qkv_w), NT, preferred_element_type=f32
+                )
+        rms = lax.rsqrt(sq / d_all + 1e-06)
+        ss[r] = rms
+        total = total * rms
+        for h in range(heads):
+            zsend[h, c, :rc] = total[:, 2 * h * hd : 2 * (h + 1) * hd].astype(bf16)
+            v_h = total[:, 2 * attn_w + h * hd : 2 * attn_w + (h + 1) * hd]
+            zsend[h, c, rc:] = jnp.concatenate([v_h[:half], v_h[half:]], axis=1).astype(bf16)
+        for dist in range(n_sp - 1, 0, -1):
+            to = lax.rem(z + dist, n_sp)
+            remote(
+                zsend.at[to, c], zrecv.at[z, c], zs_sem.at[dist, c], zr_sem.at[dist, c], {"sp": to}
+            ).start()
+        zrecv[z, c] = zsend[z, c]
+
+    pre = acc[:, qkv_w:]
+    for rel in range(2, n_tp):
+        pre = pre + lax.dot_general(
+            xs[rel], wcols(rel, qkv_w, 2 * conv_w), NT, preferred_element_type=f32
+        )
+    pre = pre * ss[...]
+    glu = (pre[:, :conv_w] * jax.nn.sigmoid(pre[:, conv_w:])).astype(bf16)
+    glu_s[...] = glu
+    taps = ck_ref.shape[0]
+    rim = halo.shape[0]
+    ext[rim:, :] = glu.astype(f32)
+    halo_copy = remote(
+        glu_s.at[pl.ds(rows - rim, rim)], halo, hs_sem, hr_sem, {"sp": lax.rem(z + 1, n_sp)}
+    )
+
+    @pl.when(z < n_sp - 1)
+    def _():
+        halo_copy.start()
+
+    @pl.when(z == 0)
+    def _():
+        halo[...] = jnp.zeros_like(halo)
+
+    @pl.when(z > 0)
+    def _():
+        halo_copy.wait_recv()
+
+    ext[:rim, :] = halo[...].astype(f32)
+
+    blk = 64
+
+    def conv_block(b, carry):
+        first = pl.multiple_of(b * blk, blk)
+        block = ext[pl.ds(first, blk + rim), :]
+        tot = jnp.zeros((blk, conv_w), f32)
+        for j in range(taps):
+            off = rim - (taps - 1) + j
+            tot = tot + block[off : off + blk] * ck_ref[j : j + 1, :].astype(f32)
+        csum[pl.ds(first, blk), :] = tot
+        return carry
+
+    lax.fori_loop(0, rows // blk, conv_block, 0)
+    cs = csum[...]
+    first = jnp.sum(cs, axis=1, keepdims=True)
+    second = jnp.sum(cs * cs, axis=1, keepdims=True)
+    lane = lax.broadcasted_iota(jnp.int32, (rows, 128), 1)
+    both = jnp.where(lane == 0, first, second)
+    st_send[...] = both.T[: st_send.shape[0]]
+    stats = []
+    for rel in range(1, n_tp):
+        cp = remote(
+            st_send, st_recv.at[rel - 1], ss_sem.at[rel], sr_sem.at[rel], {"tp": piece_owner(rel)}
+        )
+        cp.start()
+        stats.append(cp)
+    tot = st_send[...]
+    for rel in range(1, n_tp):
+        stats[rel - 1].wait_recv()
+        tot = tot + st_recv[rel - 1]
+    wide = jnp.concatenate([tot] * (128 // tot.shape[0]), axis=0).T
+    mean = wide[:, 0:1] / CONV_CH
+    var = wide[:, 1:2] / CONV_CH - mean * mean
+    normed = (csum[...] - mean) * lax.rsqrt(var + 1e-05) * lng_ref[...].astype(f32)
+    conv_out = (normed / (1.0 + jnp.exp(-normed))).astype(bf16)
+    wco_copy.wait()
+    cpart[...] = jnp.dot(conv_out, wco[...], preferred_element_type=f32)
+
+    for cp in cums:
+        cp.wait_recv()
+    for dist in range(n_sp - 1, 0, -1):
+        for c in range(AG_CHUNKS):
+            src = lax.rem(z + dist, n_sp)
+            remote(
+                zsend.at[src, c],
+                zrecv.at[src, c],
+                zs_sem.at[n_sp - dist, c],
+                zr_sem.at[n_sp - dist, c],
+                {"sp": src},
+            ).wait_recv()
+    for s in range(n_sp):
+        for c in range(AG_CHUNKS):
+            r0 = s * rows + c * rc
+            tile = zrecv[s, c, :rc].astype(f32)
+            q_s[pl.ds(r0, rc)] = tile[:, :hd].astype(bf16)
+            k_s[pl.ds(r0, rc)] = tile[:, hd:].astype(bf16)
+            vt = zrecv[s, c, rc:].astype(f32)
+            v_s[pl.ds(r0, half)] = vt[:, :hd].astype(bf16)
+            v_s[pl.ds(r0 + half, half)] = vt[:, hd:].astype(bf16)
+    scale = hd ** (-0.5)
+    hrows = rows // 2
+    for i in range(n_sp - 1, -1, -1):
+        keys = (i + 1) * rows
+        q = q_s[pl.ds(i * rows, rows)]
+        cum_k = jnp.concatenate([cum_recv[s, pl.ds(z, 1)] for s in range(i + 1)], axis=1)
+        sc = lax.dot_general(q, k_s[:keys], NT, preferred_element_type=f32) * scale - cum_k
+        q_pos = i * rows + lax.broadcasted_iota(jnp.int32, (rows, keys), 0)
+        k_pos = lax.broadcasted_iota(jnp.int32, (rows, keys), 1)
+        sc = jnp.where(k_pos <= q_pos, sc, -jnp.inf)
+        top = jnp.max(sc, axis=1, keepdims=True)
+        p = jnp.exp(sc - top)
+        tot = jnp.sum(p, axis=1, keepdims=True)
+        o = jnp.dot(p.astype(bf16), v_s[:keys], preferred_element_type=f32) / tot
+        ret_send[i] = jnp.concatenate([o[:hrows], o[hrows:]], axis=1).astype(bf16)
+        lse = jnp.broadcast_to(top + jnp.log(tot), (rows, 128)).T[:8]
+        lse_send[i] = lse + cum_recv[i, pl.ds(z, 1)]
+
+        @pl.when(z != i)
+        def _():
+            remote(
+                ret_send.at[i], ret_recv.at[z], rs_sem.at[i], rr_sem.at[z], {"sp": i}
+            ).start()
+            remote(
+                lse_send.at[i], lse_recv.at[z], ls_sem.at[i], lr_sem.at[z], {"sp": i}
+            ).start()
+
+        @pl.when(z == i)
+        def _():
+            ret_recv[i] = ret_send[i]
+            lse_recv[i] = lse_send[i]
+
+    for h in range(n_sp):
+
+        @pl.when(z != h)
+        def _():
+            remote(
+                ret_send.at[h], ret_recv.at[h], rs_sem.at[h], rr_sem.at[h], {"sp": h}
+            ).wait_recv()
+            remote(
+                lse_send.at[h], lse_recv.at[h], ls_sem.at[h], lr_sem.at[h], {"sp": h}
+            ).wait_recv()
+
+    got = [ret_recv[h].astype(f32) for h in range(n_sp)]
+    att_s[:hrows] = jnp.concatenate([g[:, :hd] for g in got], axis=1).astype(bf16)
+    att_s[hrows:] = jnp.concatenate([g[:, hd:] for g in got], axis=1).astype(bf16)
+    for h in range(n_sp):
+        log_ref[pl.ds(h, 1), :] = lse_recv[h, 0:1, :]
+    wao_copy.wait()
+
+    own_rows = rows // n_tp
+    cw = d_all // OUT_CHUNKS
+
+    def part_of(owner, n):
+        r = pl.ds(pl.multiple_of(owner * own_rows, own_rows), own_rows)
+        cols = slice(n * cw, (n + 1) * cw)
+        return cpart[r, cols] + jnp.dot(att_s[r, :], wao[:, cols], preferred_element_type=f32)
+
+    order = [dist for dist in range(1, chips)] + [0]
+    d2d = {}
+    for dist in order:
+        for n in range(OUT_CHUNKS):
+            d_send[dist, n] = part_of(other_core(dist), n).astype(bf16)
+            d2d[dist, n] = remote(
+                d_send.at[dist, n],
+                d_recv.at[dist, n],
+                ds_sem.at[dist, n],
+                dr_sem.at[dist, n],
+                {"tp": partner},
+            )
+            d2d[dist, n].start()
+    xc = {}
+    for dist in range(1, chips):
+        for n in range(OUT_CHUNKS):
+            mine = part_of(same_core(dist), n)
+            d2d[dist, n].wait_recv()
+            x_send[dist - 1, n] = (mine + d_recv[dist, n].astype(f32)).astype(bf16)
+            xc[dist, n] = remote(
+                x_send.at[dist - 1, n],
+                x_recv.at[dist - 1, n],
+                xs_sem.at[dist - 1, n],
+                xr_sem.at[dist - 1, n],
+                {"tp": same_core(dist)},
+            )
+            xc[dist, n].start()
+    for n in range(OUT_CHUNKS):
+        mine = part_of(me, n)
+        d2d[0, n].wait_recv()
+        own_part[n] = mine + d_recv[0, n].astype(f32)
+    for n in range(OUT_CHUNKS):
+        tot = own_part[n]
+        for dist in range(1, chips):
+            xc[dist, n].wait_recv()
+            tot = tot + x_recv[dist - 1, n].astype(f32)
+        out_ref[:, n * cw : (n + 1) * cw] = tot.astype(bf16)
+
+    for cp in list(ag.values()) + cums + stats + list(d2d.values()) + list(xc.values()):
+        cp.wait_send()
+
+    @pl.when(z < n_sp - 1)
+    def _():
+        halo_copy.wait_send()
+
+    for dist in range(1, n_sp):
+        to = lax.rem(z + dist, n_sp)
+        for c in range(AG_CHUNKS):
+            remote(
+                zsend.at[to, c], zrecv.at[z, c], zs_sem.at[dist, c], zr_sem.at[dist, c], {"sp": to}
+            ).wait_send()
+    for i in range(n_sp):
+
+        @pl.when(z != i)
+        def _():
+            remote(
+                ret_send.at[i], ret_recv.at[z], rs_sem.at[i], rr_sem.at[z], {"sp": i}
+            ).wait_send()
+            remote(
+                lse_send.at[i], lse_recv.at[z], ls_sem.at[i], lr_sem.at[z], {"sp": i}
+            ).wait_send()
+
+
+def fused_local(
+    n_sp,
+    n_tp,
+    inputs,
+    norm_gain,
+    w_conv_in,
+    w_conv_gate,
+    conv_kernel,
+    ln_gain,
+    w_query,
+    w_key,
+    w_value,
+    cum_gate,
+    w_conv_out,
+    w_attn_out,
+):
+    f32, bf16 = jnp.float32, jnp.bfloat16
+    rows, width = inputs.shape
+    conv_w, d_all = w_conv_in.shape
+    attn_w = w_query.shape[0]
+    heads = cum_gate.shape[0]
+    hd = attn_w // heads
+    chips = n_tp // 2
+    own_rows = rows // n_tp
+    rc = rows // AG_CHUNKS
+    rim = -(-(conv_kernel.shape[0] - 1) // 16) * 16
+    cw = d_all // OUT_CHUNKS
+    all_w = 3 * attn_w + 2 * conv_w
+    dma = pltpu.SemaphoreType.DMA
+    scratch = [
+        pltpu.VMEM((n_tp, rows, width), bf16),
+        pltpu.VMEM((n_tp, rows, width), bf16),
+        pltpu.VMEM((all_w, d_all), bf16),
+        pltpu.VMEM((conv_w, d_all), bf16),
+        pltpu.VMEM((attn_w, d_all), bf16),
+        pltpu.VMEM((rows, all_w), f32),
+        pltpu.VMEM((rows, 1), f32),
+        pltpu.VMEM((n_sp, AG_CHUNKS, rc + rc // 2, 2 * hd), bf16),
+        pltpu.VMEM((n_sp, AG_CHUNKS, rc + rc // 2, 2 * hd), bf16),
+        pltpu.VMEM((n_sp * rows, hd), bf16),
+        pltpu.VMEM((n_sp * rows, hd), bf16),
+        pltpu.VMEM((n_sp * rows, hd), bf16),
+        pltpu.VMEM((n_sp, heads, rows), f32),
+        pltpu.VMEM((rows + rim, conv_w), f32),
+        pltpu.VMEM((rows, conv_w), bf16),
+        pltpu.VMEM((rim, conv_w), bf16),
+        pltpu.VMEM((rows, conv_w), f32),
+        pltpu.VMEM((8, rows), f32),
+        pltpu.VMEM((n_tp - 1, 8, rows), f32),
+        pltpu.VMEM((rows, d_all), f32),
+        pltpu.VMEM((n_sp, rows // 2, 2 * hd), bf16),
+        pltpu.VMEM((n_sp, rows // 2, 2 * hd), bf16),
+        pltpu.VMEM((rows, attn_w), bf16),
+        pltpu.VMEM((n_sp, 8, rows), f32),
+        pltpu.VMEM((n_sp, 8, rows), f32),
+        pltpu.VMEM((chips, OUT_CHUNKS, own_rows, cw), bf16),
+        pltpu.VMEM((chips, OUT_CHUNKS, own_rows, cw), bf16),
+        pltpu.VMEM((chips - 1, OUT_CHUNKS, own_rows, cw), bf16),
+        pltpu.VMEM((chips - 1, OUT_CHUNKS, own_rows, cw), bf16),
+        pltpu.VMEM((OUT_CHUNKS, own_rows, cw), f32),
+        dma((2 * heads + 3,)),
+        dma((2,)),
+        dma,
+        dma((n_tp, AG_CHUNKS)),
+        dma((n_tp, AG_CHUNKS)),
+        dma((n_sp, AG_CHUNKS)),
+        dma((n_sp, AG_CHUNKS)),
+        dma((n_sp,)),
+        dma((n_sp,)),
+        dma,
+        dma,
+        dma((n_tp,)),
+        dma((n_tp,)),
+        dma((n_sp,)),
+        dma((n_sp,)),
+        dma((n_sp,)),
+        dma((n_sp,)),
+        dma((chips, OUT_CHUNKS)),
+        dma((chips, OUT_CHUNKS)),
+        dma((chips - 1, OUT_CHUNKS)),
+        dma((chips - 1, OUT_CHUNKS)),
+    ]
+    far = pl.BlockSpec(memory_space=pl.ANY)
+    near = pl.BlockSpec(memory_space=pltpu.VMEM)
+    mixed, log_total = pl.pallas_call(
+        functools.partial(fused_kernel, n_sp, n_tp),
+        out_shape=(
+            jax.ShapeDtypeStruct((own_rows, d_all), bf16),
+            jax.ShapeDtypeStruct((heads, rows), f32),
+        ),
+        in_specs=[far, near, far, far, near, near, far, far, far, near, far, far],
+        out_specs=(near, near),
+        scratch_shapes=scratch,
+        compiler_params=pltpu.CompilerParams(
+            collective_id=0, has_side_effects=True, vmem_limit_bytes=60 * 1024 * 1024
+        ),
+    )(
+        inputs,
+        norm_gain.reshape(1, -1),
+        w_conv_in,
+        w_conv_gate,
+        conv_kernel,
+        ln_gain.reshape(1, -1),
+        w_query,
+        w_key,
+        w_value,
+        cum_gate,
+        w_conv_out,
+        w_attn_out,
+    )
+    return (mixed, log_total)
+
+
 def solution(mesh):
     in_specs = (
         P(("grp", "sp"), "tp"),
@@ -174,4 +729,7 @@
         P("tp", None),
     )
     out_specs = (P(("grp", "sp", "tp"), None), P("tp", ("grp", "sp")))
-    return jax.shard_map(local, mesh=mesh, in_specs=in_specs, out_specs=out_specs, check_vma=False)
+    heads_here = HEADS // mesh.shape["tp"]
+    fits = heads_here == mesh.shape["sp"] and mesh.shape["tp"] % 2 == 0
+    body = functools.partial(fused_local, mesh.shape["sp"], mesh.shape["tp"]) if fits else local
+    return jax.shard_map(body, mesh=mesh, in_specs=in_specs, out_specs=out_specs, check_vma=False)

time: 144 us -> 51.1 us (0.35)
  blocking collectives: 51.9 us -> 0 us
  Pallas kernels: 0 us -> 45.3 us
  waiting for transfers between devices: 31.6 us -> 0 us
  local copies, waits for them, and re-layouts: 24.1 us -> 4.78 us
  between operations: 14.2 us -> 0.65 us
  matrix products: 8.65 us -> 0 us
  other arithmetic: 7.49 us -> 0 us
  starting transfers between devices: 3.4 us -> 0 us
  loops' own time: 2.32 us -> 0 us
    all_gather x3 -> x0, blocking collectives: 46.3 us -> none  [the longest x1 16.6 us: local(): cum_all = lax.all_gather(cum_gate.T, 'sp', axis=0, tiled=True)]
    pallas_call x0 -> x1, Pallas kernels: none -> 45.3 us  [fused_local(): pl.pallas_call(functools.partial(fused_kernel, n_sp, n_tp), out_shape=(ja...]
    reduce_scatter x1 -> x0, waiting for transfers between devices: 30.9 us -> none  [local(): lax.psum_scatter((jnp.dot(conv_out, w_conv_out, preferred_element_type=jn...]
    dot_general x5 -> x0, matrix products: 8.65 us -> none  [the longest x1 4.38 us: local(): lax.dot_general(scaled_piece, w_all, contract_dims, preferred_element_typ...]
    slice x5 -> x0, local copies, waits for them, and re-layouts: 6.18 us -> none  [the longest x2 3.24 us: local(): kernel[tap_idx][None, :]]
    psum x1 -> x0, blocking collectives: 5.67 us -> none  [local(): lax.psum((jnp.sum(conv_sum, axis=1), jnp.sum(conv_sum * conv_sum, axis=1)...]
    dynamic_slice x4 -> x0, local copies, waits for them, and re-layouts: 4.92 us -> none  [local(): lax.scan(visit, state, (k_split, v_split, jnp.arange(block_count, dtype=j...]
    reduce_sum x3 -> x0, other arithmetic: 4.74 us -> none  [the longest x1 3.07 us: local(): jnp.sum(conv_sum, axis=1)]
  transfers between devices with their start and end apart: 3 -> 0, of which waited for: 1 -> 0; matrix products, arithmetic and copies ran while one was open for 19% -> 0% of each run, Pallas kernels for 0% -> 0%
where the time goes in v1:
time: 51.1 us; the launch traced here: 50.8 us
  Pallas kernels  45.3 us (89%)
  local copies, waits for them, and re-layouts  4.78 us (9%)
  between operations  0.65 us (1%)
    pallas_call x1, Pallas kernels, fused_local(): pl.pallas_call(functools.partial(fused_kernel, n_sp, n_tp), out_shape=(ja...  45.3 us
    unnamed x4, local copies, waits for them, and re-layouts  2.27 us
    reshape x1, local copies, waits for them, and re-layouts, fused_local(): norm_gain.reshape(1, -1)  1.29 us
    reshape x1, local copies, waits for them, and re-layouts, fused_local(): ln_gain.reshape(1, -1)  1.22 us

profile of v1, /device:TPU:0, one launch (start us, length us, event | category | flops | bytes accessed | tf_op | source)
XLA Modules:
  0.0 50.8 jit_solution(3881719258938930086)
XLA Ops:
  0.6 1.2 %reshape.11.lng_ref = bf16[1,256]{1,0:T(2,128)(2,1)} reshape(bf16[256]{0:T(256)(128)(2,1)} %param.17) | data formatting | bytes 1024 | tf_op jit(solution)/shard_map/reshape | solution.py:705
  1.9 1.3 %reshape.10.gain_ref = bf16[1,2048]{1,0:T(2,128)(2,1)} reshape(bf16[2048]{0:T(1024)(128)(2,1)} %param.13) | data formatting | bytes 8192 | tf_op jit(solution)/shard_map/reshape | solution.py:701
  3.1 45.3 %shard_map.131 = (bf16[64,2048]{1,0:T(8,128)(2,1)}, f32[4,256]{1,0:T(4,128)}) custom-call(bf16[256,512]{1,0:T(8,128)(2,1)} %x_hbm.1, bf16[1,2048]{1,0:T(2,128)(2,1)} %reshape.10.gain_ref, bf16[256,2048]{1,0:T(8,128)(2,1)} %wci_hbm.1, bf16[256,2048]{1,0:T(8,128)(2,1)} %wcg_hbm.1, bf16[31,256]{1,0:T(8,128)(2,1)} %ck_ref.1, bf16[1,256]{1,0:T(2,128)(2,1)} %reshape.11.lng_ref, ...), custom_call_target="tpu_custom_call" | custom-call | tf_op jit(solution)/shard_map/pallas_call | solution.py:687
  48.5 0.0 copy-start
  48.5 1.7 %copy.16 = bf16[64,2048]{1,0:T(8,128)(2,1)} copy(bf16[64,2048]{1,0:T(8,128)(2,1)} %get-tuple-element.4) | data formatting | bytes 524288
  50.2 0.0 copy-done
  50.2 0.6 %copy.17 = f32[4,256]{1,0:T(4,128)} copy(f32[4,256]{1,0:T(4,128)S(1)} %copy-done) | data formatting | bytes 8192
Async XLA Ops:
  48.5 1.7 %copy-start = (f32[4,256]{1,0:T(4,128)S(1)}, f32[4,256]{1,0:T(4,128)}, u32[]{:S(2)}) copy-start(f32[4,256]{1,0:T(4,128)} %get-tuple-element.5) | copy-start | bytes 12292

commit v2 on v1

--- a/solution.py
+++ b/solution.py
@@ -214,7 +214,7 @@
     d_recv,
     x_send,
     x_recv,
-    own_part,
+    parts,
     wsem,
     owsem,
     xsem,
@@ -335,7 +335,7 @@
         r = pl.ds(c0, n)
         owner = piece_source(rel)
         raw = xg[rel, r].astype(f32)
-        g = gain_ref[:, pl.ds(pl.multiple_of(owner * width, width), width)].astype(f32)
+        g = gain_ref[pl.ds(pl.multiple_of(owner * width, width), width)].astype(f32).reshape(1, width)
         xs[rel, r] = (raw * g).astype(bf16)
         return jnp.sum(raw * raw, axis=1, keepdims=True)
 
@@ -398,10 +398,9 @@
         )
     pre = pre * ss[...]
     glu = (pre[:, :conv_w] * jax.nn.sigmoid(pre[:, conv_w:])).astype(bf16)
-    glu_s[...] = glu
     taps = ck_ref.shape[0]
     rim = halo.shape[0]
-    ext[rim:, :] = glu.astype(f32)
+    glu_s[...] = glu
     halo_copy = remote(
         glu_s.at[pl.ds(rows - rim, rim)], halo, hs_sem, hr_sem, {"sp": lax.rem(z + 1, n_sp)}
     )
@@ -410,16 +409,7 @@
     def _():
         halo_copy.start()
 
-    @pl.when(z == 0)
-    def _():
-        halo[...] = jnp.zeros_like(halo)
-
-    @pl.when(z > 0)
-    def _():
-        halo_copy.wait_recv()
-
-    ext[:rim, :] = halo[...].astype(f32)
-
+    ext[rim:, :] = glu.astype(f32)
     blk = 64
 
     def conv_block(b, carry):
@@ -432,7 +422,73 @@
         csum[pl.ds(first, blk), :] = tot
         return carry
 
-    lax.fori_loop(0, rows // blk, conv_block, 0)
+    lax.fori_loop(1, rows // blk, conv_block, 0)
+    for cp in cums:
+        cp.wait_recv()
+    for dist in range(n_sp - 1, 0, -1):
+        for c in range(AG_CHUNKS):
+            src = lax.rem(z + dist, n_sp)
+            remote(
+                zsend.at[src, c],
+                zrecv.at[src, c],
+                zs_sem.at[n_sp - dist, c],
+                zr_sem.at[n_sp - dist, c],
+                {"sp": src},
+            ).wait_recv()
+    for s in range(n_sp):
+        for c in range(AG_CHUNKS):
+            r0 = s * rows + c * rc
+            tile = zrecv[s, c, :rc].astype(f32)
+            q_s[pl.ds(r0, rc)] = tile[:, :hd].astype(bf16)
+            k_s[pl.ds(r0, rc)] = tile[:, hd:].astype(bf16)
+            vt = zrecv[s, c, rc:].astype(f32)
+            v_s[pl.ds(r0, half)] = vt[:, :hd].astype(bf16)
+            v_s[pl.ds(r0 + half, half)] = vt[:, hd:].astype(bf16)
+    scale = hd ** (-0.5)
+    hrows = rows // 2
+    allowed = lax.broadcasted_iota(jnp.int32, (rows, rows), 1) <= lax.broadcasted_iota(
+        jnp.int32, (rows, rows), 0
+    )
+    for i in range(n_sp - 1, -1, -1):
+        keys = (i + 1) * rows
+        q = q_s[pl.ds(i * rows, rows)]
+        cum_k = jnp.concatenate([cum_recv[s, pl.ds(z, 1)] for s in range(i + 1)], axis=1)
+        sc = lax.dot_general(q, k_s[:keys], NT, preferred_element_type=f32) * scale - cum_k
+        diag = jnp.where(allowed, sc[:, keys - rows :], -jnp.inf)
+        sc = diag if i == 0 else jnp.concatenate([sc[:, : keys - rows], diag], axis=1)
+        top = jnp.max(sc, axis=1, keepdims=True)
+        p = jnp.exp(sc - top)
+        tot = jnp.sum(p, axis=1, keepdims=True)
+        o = jnp.dot(p.astype(bf16), v_s[:keys], preferred_element_type=f32) / tot
+        ret_send[i] = jnp.concatenate([o[:hrows], o[hrows:]], axis=1).astype(bf16)
+        lse = jnp.broadcast_to(top + jnp.log(tot), (rows, 128)).T[:8]
+        lse_send[i] = lse + cum_recv[i, pl.ds(z, 1)]
+
+        @pl.when(z != i)
+        def _():
+            remote(
+                ret_send.at[i], ret_recv.at[z], rs_sem.at[i], rr_sem.at[z], {"sp": i}
+            ).start()
+            remote(
+                lse_send.at[i], lse_recv.at[z], ls_sem.at[i], lr_sem.at[z], {"sp": i}
+            ).start()
+
+        @pl.when(z == i)
+        def _():
+            ret_recv[i] = ret_send[i]
+            lse_recv[i] = lse_send[i]
+
+
+    @pl.when(z == 0)
+    def _():
+        halo[...] = jnp.zeros_like(halo)
+
+    @pl.when(z > 0)
+    def _():
+        halo_copy.wait_recv()
+
+    ext[:rim, :] = halo[...].astype(f32)
+    conv_block(0, 0)
     cs = csum[...]
     first = jnp.sum(cs, axis=1, keepdims=True)
     second = jnp.sum(cs * cs, axis=1, keepdims=True)
@@ -453,63 +509,10 @@
     wide = jnp.concatenate([tot] * (128 // tot.shape[0]), axis=0).T
     mean = wide[:, 0:1] / CONV_CH
     var = wide[:, 1:2] / CONV_CH - mean * mean
-    normed = (csum[...] - mean) * lax.rsqrt(var + 1e-05) * lng_ref[...].astype(f32)
+    normed = (csum[...] - mean) * lax.rsqrt(var + 1e-05) * lng_ref[...].astype(f32).reshape(1, conv_w)
     conv_out = (normed / (1.0 + jnp.exp(-normed))).astype(bf16)
     wco_copy.wait()
     cpart[...] = jnp.dot(conv_out, wco[...], preferred_element_type=f32)
-
-    for cp in cums:
-        cp.wait_recv()
-    for dist in range(n_sp - 1, 0, -1):
-        for c in range(AG_CHUNKS):
-            src = lax.rem(z + dist, n_sp)
-            remote(
-                zsend.at[src, c],
-                zrecv.at[src, c],
-                zs_sem.at[n_sp - dist, c],
-                zr_sem.at[n_sp - dist, c],
-                {"sp": src},
-            ).wait_recv()
-    for s in range(n_sp):
-        for c in range(AG_CHUNKS):
-            r0 = s * rows + c * rc
-            tile = zrecv[s, c, :rc].astype(f32)
-            q_s[pl.ds(r0, rc)] = tile[:, :hd].astype(bf16)
-            k_s[pl.ds(r0, rc)] = tile[:, hd:].astype(bf16)
-            vt = zrecv[s, c, rc:].astype(f32)
-            v_s[pl.ds(r0, half)] = vt[:, :hd].astype(bf16)
-            v_s[pl.ds(r0 + half, half)] = vt[:, hd:].astype(bf16)
-    scale = hd ** (-0.5)
-    hrows = rows // 2
-    for i in range(n_sp - 1, -1, -1):
-        keys = (i + 1) * rows
-        q = q_s[pl.ds(i * rows, rows)]
-        cum_k = jnp.concatenate([cum_recv[s, pl.ds(z, 1)] for s in range(i + 1)], axis=1)
-        sc = lax.dot_general(q, k_s[:keys], NT, preferred_element_type=f32) * scale - cum_k
-        q_pos = i * rows + lax.broadcasted_iota(jnp.int32, (rows, keys), 0)
-        k_pos = lax.broadcasted_iota(jnp.int32, (rows, keys), 1)
-        sc = jnp.where(k_pos <= q_pos, sc, -jnp.inf)
-        top = jnp.max(sc, axis=1, keepdims=True)
-        p = jnp.exp(sc - top)
-        tot = jnp.sum(p, axis=1, keepdims=True)
-        o = jnp.dot(p.astype(bf16), v_s[:keys], preferred_element_type=f32) / tot
-        ret_send[i] = jnp.concatenate([o[:hrows], o[hrows:]], axis=1).astype(bf16)
-        lse = jnp.broadcast_to(top + jnp.log(tot), (rows, 128)).T[:8]
-        lse_send[i] = lse + cum_recv[i, pl.ds(z, 1)]
-
-        @pl.when(z != i)
-        def _():
-            remote(
-                ret_send.at[i], ret_recv.at[z], rs_sem.at[i], rr_sem.at[z], {"sp": i}
-            ).start()
-            remote(
-                lse_send.at[i], lse_recv.at[z], ls_sem.at[i], lr_sem.at[z], {"sp": i}
-            ).start()
-
-        @pl.when(z == i)
-        def _():
-            ret_recv[i] = ret_send[i]
-            lse_recv[i] = lse_send[i]
 
     for h in range(n_sp):
 
@@ -528,20 +531,21 @@
     for h in range(n_sp):
         log_ref[pl.ds(h, 1), :] = lse_recv[h, 0:1, :]
     wao_copy.wait()
-
     own_rows = rows // n_tp
     cw = d_all // OUT_CHUNKS
-
-    def part_of(owner, n):
-        r = pl.ds(pl.multiple_of(owner * own_rows, own_rows), own_rows)
-        cols = slice(n * cw, (n + 1) * cw)
-        return cpart[r, cols] + jnp.dot(att_s[r, :], wao[:, cols], preferred_element_type=f32)
-
-    order = [dist for dist in range(1, chips)] + [0]
-    d2d = {}
-    for dist in order:
+    mine = pl.ds(pl.multiple_of(core * own_rows, own_rows), own_rows)
+    theirs = pl.ds(pl.multiple_of((1 - core) * own_rows, own_rows), own_rows)
+    d2d, xc = {}, {}
+
+    def exchange(dist):
+        to_chip = lax.rem(chip + dist, chips)
+        r = pl.ds(pl.multiple_of(to_chip * 2 * own_rows, 2 * own_rows), 2 * own_rows)
         for n in range(OUT_CHUNKS):
-            d_send[dist, n] = part_of(other_core(dist), n).astype(bf16)
+            cols = slice(n * cw, (n + 1) * cw)
+            parts[dist, n] = cpart[r, cols] + jnp.dot(
+                att_s[r, :], wao[:, cols], preferred_element_type=f32
+            )
+            d_send[dist, n] = parts[dist, n, theirs].astype(bf16)
             d2d[dist, n] = remote(
                 d_send.at[dist, n],
                 d_recv.at[dist, n],
@@ -550,12 +554,13 @@
                 {"tp": partner},
             )
             d2d[dist, n].start()
-    xc = {}
-    for dist in range(1, chips):
+
+    def forward(dist):
         for n in range(OUT_CHUNKS):
-            mine = part_of(same_core(dist), n)
             d2d[dist, n].wait_recv()
-            x_send[dist - 1, n] = (mine + d_recv[dist, n].astype(f32)).astype(bf16)
+            x_send[dist - 1, n] = (
+                parts[dist, n, mine] + d_recv[dist, n].astype(f32)
+            ).astype(bf16)
             xc[dist, n] = remote(
                 x_send.at[dist - 1, n],
                 x_recv.at[dist - 1, n],
@@ -564,12 +569,16 @@
                 {"tp": same_core(dist)},
             )
             xc[dist, n].start()
+
+    for dist in range(1, chips):
+        exchange(dist)
+    for dist in range(1, chips):
+        forward(dist)
+    exchange(0)
     for n in range(OUT_CHUNKS):
-        mine = part_of(me, n)
         d2d[0, n].wait_recv()
-        own_part[n] = mine + d_recv[0, n].astype(f32)
     for n in range(OUT_CHUNKS):
-        tot = own_part[n]
+        tot = parts[0, n, mine] + d_recv[0, n].astype(f32)
         for dist in range(1, chips):
             xc[dist, n].wait_recv()
             tot = tot + x_recv[dist - 1, n].astype(f32)
@@ -659,7 +668,7 @@
         pltpu.VMEM((chips, OUT_CHUNKS, own_rows, cw), bf16),
         pltpu.VMEM((chips - 1, OUT_CHUNKS, own_rows, cw), bf16),
         pltpu.VMEM((chips - 1, OUT_CHUNKS, own_rows, cw), bf16),
-        pltpu.VMEM((OUT_CHUNKS, own_rows, cw), f32),
+        pltpu.VMEM((chips, OUT_CHUNKS, 2 * own_rows, cw), f32),
         dma((2 * heads + 3,)),
         dma((2,)),
         dma,
@@ -687,8 +696,8 @@
     mixed, log_total = pl.pallas_call(
         functools.partial(fused_kernel, n_sp, n_tp),
         out_shape=(
-            jax.ShapeDtypeStruct((own_rows, d_all), bf16),
-            jax.ShapeDtypeStruct((heads, rows), f32),
+            pltpu.VMEM((own_rows, d_all), bf16),
+            pltpu.VMEM((heads, rows), f32),
         ),
         in_specs=[far, near, far, far, near, near, far, far, far, near, far, far],
         out_specs=(near, near),
@@ -698,11 +707,11 @@
         ),
     )(
         inputs,
-        norm_gain.reshape(1, -1),
+        norm_gain,
         w_conv_in,
         w_conv_gate,
         conv_kernel,
-        ln_gain.reshape(1, -1),
+        ln_gain,
         w_query,
         w_key,
         w_value,

time: 51.1 us -> 42.4 us (0.83)
  Pallas kernels: 45.3 us -> 40.2 us
  local copies, waits for them, and re-layouts: 4.78 us -> 1.3 us
    pallas_call x1, Pallas kernels: 45.3 us -> 40.2 us  [fused_local(): pl.pallas_call(functools.partial(fused_kernel, n_sp, n_tp), out_shape=(pl...]
    reshape x2 -> x0, local copies, waits for them, and re-layouts: 2.51 us -> none  [the longest x1 1.29 us: fused_local(): norm_gain.reshape(1, -1)]
    unnamed x4 -> x2, local copies, waits for them, and re-layouts: 2.27 us -> 1.3 us
where the time goes in v2:
time: 42.4 us; the launch traced here: 42.1 us
  Pallas kernels  40.2 us (95%)
  local copies, waits for them, and re-layouts  1.3 us (3%)
  between operations  0.64 us (2%)
    pallas_call x1, Pallas kernels, fused_local(): pl.pallas_call(functools.partial(fused_kernel, n_sp, n_tp), out_shape=(pl...  40.2 us
    unnamed x2, local copies, waits for them, and re-layouts  1.3 us

profile of v2, /device:TPU:0, one launch (start us, length us, event | category | flops | bytes accessed | tf_op | source)
XLA Modules:
  0.0 42.1 jit_solution(16883041009299010512)
XLA Ops:
  0.6 40.2 %shard_map.131 = (bf16[64,2048]{1,0:T(8,128)(2,1)S(1)}, f32[4,256]{1,0:T(4,128)S(1)}) custom-call(bf16[256,512]{1,0:T(8,128)(2,1)} %x_hbm.1, bf16[2048]{0:T(1024)(128)(2,1)} %gain_ref.1, bf16[256,2048]{1,0:T(8,128)(2,1)} %wci_hbm.1, bf16[256,2048]{1,0:T(8,128)(2,1)} %wcg_hbm.1, bf16[31,256]{1,0:T(8,128)(2,1)} %ck_ref.1, bf16[256]{0:T(256)(128)(2,1)} %lng_ref.1, ...), custom_call_target="tpu_custom_call" | custom-call | tf_op jit(solution)/shard_map/pallas_call | solution.py:696
  40.8 0.7 %copy.16 = bf16[64,2048]{1,0:T(8,128)(2,1)} copy(bf16[64,2048]{1,0:T(8,128)(2,1)S(1)} %get-tuple-element.2) | data formatting | bytes 524288
  41.5 0.6 %copy.17 = f32[4,256]{1,0:T(4,128)} copy(f32[4,256]{1,0:T(4,128)S(1)} %get-tuple-element.3) | data formatting | bytes 8192

commit v3 on v2

--- a/solution.py
+++ b/solution.py
@@ -162,7 +162,7 @@
     return (mixed, log_total)
 
 
-AG_CHUNKS = 4
+AG_CHUNKS = 8
 OUT_CHUNKS = 4
 MESH = pl.DeviceIdType.MESH
 NT = (((1,), (1,)), ((), ()))
@@ -197,9 +197,11 @@
     q_s,
     k_s,
     v_s,
+    v_t,
+    cum_col,
     cum_recv,
     ext,
-    glu_s,
+    halo_src,
     halo,
     csum,
     st_send,
@@ -313,12 +315,13 @@
             {"tp": partner},
         )
 
+    order = [AG_CHUNKS - 1] + list(range(AG_CHUNKS - 1))
     ag = {}
-    for c in range(AG_CHUNKS):
+    for c in order:
         for dist in range(1, chips):
             ag[2 * dist, c] = ag_copy(2 * dist, "own", c)
             ag[2 * dist, c].start()
-    for c in range(AG_CHUNKS):
+    for c in order:
         ag[1, c] = ag_copy(1, "own", c)
         ag[1, c].start()
     cums = []
@@ -361,22 +364,20 @@
     )
 
     half = rc // 2
-    for c in range(AG_CHUNKS):
+
+    def finish_chunk(c):
         r = pl.ds(c * rc, rc)
-        for dist in range(1, chips):
-            ag[2 * dist, c].wait_recv()
-            ag[2 * dist + 1, c] = ag_copy(2 * dist + 1, "relay", c)
-            ag[2 * dist + 1, c].start()
         total = acc[r, :qkv_w]
         sq = ss[r]
         for dist in range(1, chips):
-            for rel in (2 * dist, 2 * dist + 1):
-                if rel % 2 == 1:
-                    ag[rel, c].wait_recv()
-                sq = sq + prepare(rel, c * rc, rc)
-                total = total + lax.dot_general(
-                    xs[rel, r], wcols(rel, 0, qkv_w), NT, preferred_element_type=f32
-                )
+            ag[2 * dist + 1, c].wait_recv()
+            sq = sq + prepare(2 * dist + 1, c * rc, rc)
+            total = total + lax.dot_general(
+                xs[2 * dist + 1, r],
+                wcols(2 * dist + 1, 0, qkv_w),
+                NT,
+                preferred_element_type=f32,
+            )
         rms = lax.rsqrt(sq / d_all + 1e-06)
         ss[r] = rms
         total = total * rms
@@ -391,24 +392,46 @@
             ).start()
         zrecv[z, c] = zsend[z, c]
 
-    pre = acc[:, qkv_w:]
-    for rel in range(2, n_tp):
-        pre = pre + lax.dot_general(
-            xs[rel], wcols(rel, qkv_w, 2 * conv_w), NT, preferred_element_type=f32
-        )
-    pre = pre * ss[...]
-    glu = (pre[:, :conv_w] * jax.nn.sigmoid(pre[:, conv_w:])).astype(bf16)
+    rim = halo.shape[0]
+    halo_copy = remote(
+        halo_src, halo, hs_sem, hr_sem, {"sp": lax.rem(z + 1, n_sp)}
+    )
+
+    def gated(r):
+        pre = acc[r, qkv_w:]
+        for rel in range(2, n_tp):
+            pre = pre + lax.dot_general(
+                xs[rel, r], wcols(rel, qkv_w, 2 * conv_w), NT, preferred_element_type=f32
+            )
+        pre = pre * ss[r]
+        return (pre[:, :conv_w] * jax.nn.sigmoid(pre[:, conv_w:])).astype(bf16)
+
+    for k, c in enumerate(order):
+        r = pl.ds(c * rc, rc)
+        for dist in range(1, chips):
+            ag[2 * dist, c].wait_recv()
+            ag[2 * dist + 1, c] = ag_copy(2 * dist + 1, "relay", c)
+            ag[2 * dist + 1, c].start()
+        for dist in range(1, chips):
+            ss[r] += prepare(2 * dist, c * rc, rc)
+            acc[r, :qkv_w] += lax.dot_general(
+                xs[2 * dist, r], wcols(2 * dist, 0, qkv_w), NT, preferred_element_type=f32
+            )
+        if k == 0:
+            finish_chunk(c)
+        elif k == 1:
+            halo_src[...] = gated(pl.ds(rows - rim, rim))
+
+            @pl.when(z < n_sp - 1)
+            def _():
+                halo_copy.start()
+
+        else:
+            finish_chunk(order[k - 1])
+    finish_chunk(order[-1])
+
+    glu = gated(pl.ds(0, rows))
     taps = ck_ref.shape[0]
-    rim = halo.shape[0]
-    glu_s[...] = glu
-    halo_copy = remote(
-        glu_s.at[pl.ds(rows - rim, rim)], halo, hs_sem, hr_sem, {"sp": lax.rem(z + 1, n_sp)}
-    )
-
-    @pl.when(z < n_sp - 1)
-    def _():
-        halo_copy.start()
-
     ext[rim:, :] = glu.astype(f32)
     blk = 64
 
@@ -425,59 +448,10 @@
     lax.fori_loop(1, rows // blk, conv_block, 0)
     for cp in cums:
         cp.wait_recv()
-    for dist in range(n_sp - 1, 0, -1):
-        for c in range(AG_CHUNKS):
-            src = lax.rem(z + dist, n_sp)
-            remote(
-                zsend.at[src, c],
-                zrecv.at[src, c],
-                zs_sem.at[n_sp - dist, c],
-                zr_sem.at[n_sp - dist, c],
-                {"sp": src},
-            ).wait_recv()
-    for s in range(n_sp):
-        for c in range(AG_CHUNKS):
-            r0 = s * rows + c * rc
-            tile = zrecv[s, c, :rc].astype(f32)
-            q_s[pl.ds(r0, rc)] = tile[:, :hd].astype(bf16)
-            k_s[pl.ds(r0, rc)] = tile[:, hd:].astype(bf16)
-            vt = zrecv[s, c, rc:].astype(f32)
-            v_s[pl.ds(r0, half)] = vt[:, :hd].astype(bf16)
-            v_s[pl.ds(r0 + half, half)] = vt[:, hd:].astype(bf16)
-    scale = hd ** (-0.5)
-    hrows = rows // 2
-    allowed = lax.broadcasted_iota(jnp.int32, (rows, rows), 1) <= lax.broadcasted_iota(
-        jnp.int32, (rows, rows), 0
-    )
-    for i in range(n_sp - 1, -1, -1):
-        keys = (i + 1) * rows
-        q = q_s[pl.ds(i * rows, rows)]
-        cum_k = jnp.concatenate([cum_recv[s, pl.ds(z, 1)] for s in range(i + 1)], axis=1)
-        sc = lax.dot_general(q, k_s[:keys], NT, preferred_element_type=f32) * scale - cum_k
-        diag = jnp.where(allowed, sc[:, keys - rows :], -jnp.inf)
-        sc = diag if i == 0 else jnp.concatenate([sc[:, : keys - rows], diag], axis=1)
-        top = jnp.max(sc, axis=1, keepdims=True)
-        p = jnp.exp(sc - top)
-        tot = jnp.sum(p, axis=1, keepdims=True)
-        o = jnp.dot(p.astype(bf16), v_s[:keys], preferred_element_type=f32) / tot
-        ret_send[i] = jnp.concatenate([o[:hrows], o[hrows:]], axis=1).astype(bf16)
-        lse = jnp.broadcast_to(top + jnp.log(tot), (rows, 128)).T[:8]
-        lse_send[i] = lse + cum_recv[i, pl.ds(z, 1)]
-
-        @pl.when(z != i)
-        def _():
-            remote(
-                ret_send.at[i], ret_recv.at[z], rs_sem.at[i], rr_sem.at[z], {"sp": i}
-            ).start()
-            remote(
-                lse_send.at[i], lse_recv.at[z], ls_sem.at[i], lr_sem.at[z], {"sp": i}
-            ).start()
-
-        @pl.when(z == i)
-        def _():
-            ret_recv[i] = ret_send[i]
-            lse_recv[i] = lse_send[i]
-
+    for src in range(n_sp):
+        cum_col[pl.ds(src * rows, rows)] = jnp.broadcast_to(
+            cum_recv[src, pl.ds(z, 1)], (128, rows)
+        ).T
 
     @pl.when(z == 0)
     def _():
@@ -502,6 +476,61 @@
         )
         cp.start()
         stats.append(cp)
+    for dist in range(n_sp - 1, 0, -1):
+        for c in range(AG_CHUNKS):
+            src = lax.rem(z + dist, n_sp)
+            remote(
+                zsend.at[src, c],
+                zrecv.at[src, c],
+                zs_sem.at[n_sp - dist, c],
+                zr_sem.at[n_sp - dist, c],
+                {"sp": src},
+            ).wait_recv()
+    scale = hd ** (-0.5)
+    low = lax.broadcasted_iota(jnp.int32, (half, 2 * hd), 1) < hd
+    for s in range(n_sp):
+        for c in range(AG_CHUNKS):
+            r0 = s * rows + c * rc
+            tile = zrecv[s, c, :rc].astype(f32)
+            q_s[pl.ds(r0, rc)] = (tile[:, :hd] * scale).astype(bf16)
+            k_s[pl.ds(r0, rc)] = tile[:, hd:].astype(bf16)
+            vt = zrecv[s, c, rc:].astype(f32)
+            v_s[pl.ds(r0, half)] = jnp.where(low, vt, 1.0).astype(bf16)
+            v_s[pl.ds(r0 + half, half)] = jnp.where(low, pltpu.roll(vt, hd, 1), 1.0).astype(bf16)
+    v_t[...] = v_s[...].T
+    wide_k = -(-rows // 128)
+    allowed = lax.broadcasted_iota(jnp.int32, (rows, rows), 0) <= lax.broadcasted_iota(
+        jnp.int32, (rows, rows), 1
+    )
+    for i in [k // 2 if k % 2 == 0 else n_sp - 1 - k // 2 for k in range(n_sp)]:
+        keys = (i + 1) * rows
+        q = q_s[pl.ds(i * rows, rows)]
+        cum_k = jnp.concatenate([cum_col[:keys]] * wide_k, axis=1)
+        sc = lax.dot_general(k_s[:keys], q, NT, preferred_element_type=f32) - cum_k
+        diag = jnp.where(allowed, sc[keys - rows :], -jnp.inf)
+        sc = diag if i == 0 else jnp.concatenate([sc[: keys - rows], diag], axis=0)
+        top = jnp.max(sc, axis=0, keepdims=True)
+        p = jnp.exp(sc - top).astype(bf16)
+        both = jnp.dot(v_t[:, :keys], p, preferred_element_type=f32)
+        tot = both[hd : hd + 1]
+        ret_send[i] = (both[:hd] / tot).astype(bf16)
+        lse = top + jnp.log(tot) + cum_recv[i, pl.ds(z, 1)]
+        lse_send[i] = jnp.broadcast_to(lse, (8, rows))
+
+        @pl.when(z != i)
+        def _():
+            remote(
+                ret_send.at[i], ret_recv.at[z], rs_sem.at[i], rr_sem.at[z], {"sp": i}
+            ).start()
+            remote(
+                lse_send.at[i], lse_recv.at[z], ls_sem.at[i], lr_sem.at[z], {"sp": i}
+            ).start()
+
+        @pl.when(z == i)
+        def _():
+            ret_recv[i] = ret_send[i]
+            lse_recv[i] = lse_send[i]
+
     tot = st_send[...]
     for rel in range(1, n_tp):
         stats[rel - 1].wait_recv()
@@ -525,9 +554,7 @@
                 lse_send.at[h], lse_recv.at[h], ls_sem.at[h], lr_sem.at[h], {"sp": h}
             ).wait_recv()
 
-    got = [ret_recv[h].astype(f32) for h in range(n_sp)]
-    att_s[:hrows] = jnp.concatenate([g[:, :hd] for g in got], axis=1).astype(bf16)
-    att_s[hrows:] = jnp.concatenate([g[:, hd:] for g in got], axis=1).astype(bf16)
+    att_s[...] = jnp.concatenate([ret_recv[h] for h in range(n_sp)], axis=0).astype(f32).T.astype(bf16)
     for h in range(n_sp):
         log_ref[pl.ds(h, 1), :] = lse_recv[h, 0:1, :]
     wao_copy.wait()
@@ -650,17 +677,19 @@
         pltpu.VMEM((n_sp, AG_CHUNKS, rc + rc // 2, 2 * hd), bf16),
         pltpu.VMEM((n_sp * rows, hd), bf16),
         pltpu.VMEM((n_sp * rows, hd), bf16),
-        pltpu.VMEM((n_sp * rows, hd), bf16),
+        pltpu.VMEM((n_sp * rows, 2 * hd), bf16),
+        pltpu.VMEM((2 * hd, n_sp * rows), bf16),
+        pltpu.VMEM((n_sp * rows, 128), f32),
         pltpu.VMEM((n_sp, heads, rows), f32),
         pltpu.VMEM((rows + rim, conv_w), f32),
-        pltpu.VMEM((rows, conv_w), bf16),
+        pltpu.VMEM((rim, conv_w), bf16),
         pltpu.VMEM((rim, conv_w), bf16),
         pltpu.VMEM((rows, conv_w), f32),
         pltpu.VMEM((8, rows), f32),
         pltpu.VMEM((n_tp - 1, 8, rows), f32),
         pltpu.VMEM((rows, d_all), f32),
-        pltpu.VMEM((n_sp, rows // 2, 2 * hd), bf16),
-        pltpu.VMEM((n_sp, rows // 2, 2 * hd), bf16),
+        pltpu.VMEM((n_sp, hd, rows), bf16),
+        pltpu.VMEM((n_sp, hd, rows), bf16),
         pltpu.VMEM((rows, attn_w), bf16),
         pltpu.VMEM((n_sp, 8, rows), f32),
         pltpu.VMEM((n_sp, 8, rows), f32),

time: 42.4 us -> 39.8 us (0.939)
  Pallas kernels: 40.2 us -> 37.6 us
    pallas_call x1, Pallas kernels: 40.2 us -> 37.6 us  [fused_local(): pl.pallas_call(functools.partial(fused_kernel, n_sp, n_tp), out_shape=(pl...]
where the time goes in v3:
time: 39.8 us; the launch traced here: 39.5 us
  Pallas kernels  37.6 us (94%)
  local copies, waits for them, and re-layouts  1.3 us (3%)
  between operations  0.64 us (2%)
    pallas_call x1, Pallas kernels, fused_local(): pl.pallas_call(functools.partial(fused_kernel, n_sp, n_tp), out_shape=(pl...  37.6 us
    unnamed x2, local copies, waits for them, and re-layouts  1.3 us

profile of v3, /device:TPU:0, one launch (start us, length us, event | category | flops | bytes accessed | tf_op | source)
XLA Modules:
  0.0 39.5 jit_solution(6736771993719133091)
XLA Ops:
  0.6 37.6 %shard_map.131 = (bf16[64,2048]{1,0:T(8,128)(2,1)S(1)}, f32[4,256]{1,0:T(4,128)S(1)}) custom-call(bf16[256,512]{1,0:T(8,128)(2,1)} %x_hbm.1, bf16[2048]{0:T(1024)(128)(2,1)} %gain_ref.1, bf16[256,2048]{1,0:T(8,128)(2,1)} %wci_hbm.1, bf16[256,2048]{1,0:T(8,128)(2,1)} %wcg_hbm.1, bf16[31,256]{1,0:T(8,128)(2,1)} %ck_ref.1, bf16[256]{0:T(256)(128)(2,1)} %lng_ref.1, ...), custom_call_target="tpu_custom_call" | custom-call | tf_op jit(solution)/shard_map/pallas_call | solution.py:725
  38.2 0.7 %copy.16 = bf16[64,2048]{1,0:T(8,128)(2,1)} copy(bf16[64,2048]{1,0:T(8,128)(2,1)S(1)} %get-tuple-element.2) | data formatting | bytes 524288
  38.9 0.6 %copy.17 = f32[4,256]{1,0:T(4,128)} copy(f32[4,256]{1,0:T(4,128)S(1)} %get-tuple-element.3) | data formatting | bytes 8192

commit v4 on v3

--- a/solution.py
+++ b/solution.py
@@ -198,6 +198,8 @@
     k_s,
     v_s,
     v_t,
+    out_loc,
+    lse_loc,
     cum_col,
     cum_recv,
     ext,
@@ -284,9 +286,9 @@
     own_copy.start()
     loads = []
     for h in range(heads):
-        loads.append((wq_hbm.at[pl.ds(h * hd, hd)], wbuf.at[pl.ds(2 * h * hd, hd)]))
-        loads.append((wk_hbm.at[pl.ds(h * hd, hd)], wbuf.at[pl.ds((2 * h + 1) * hd, hd)]))
-    loads.append((wv_hbm, wbuf.at[pl.ds(2 * attn_w, attn_w)]))
+        loads.append((wk_hbm.at[pl.ds(h * hd, hd)], wbuf.at[pl.ds(2 * h * hd, hd)]))
+        loads.append((wv_hbm.at[pl.ds(h * hd, hd)], wbuf.at[pl.ds((2 * h + 1) * hd, hd)]))
+    loads.append((wq_hbm, wbuf.at[pl.ds(2 * attn_w, attn_w)]))
     qkv_loads = len(loads)
     qkv_w = 3 * attn_w
     loads.append((wci_hbm, wbuf.at[pl.ds(qkv_w, conv_w)]))
@@ -364,6 +366,27 @@
     )
 
     half = rc // 2
+    spans = (pl.ds(0, rc), pl.ds(rc, half))
+
+    def z_copy(dist, c, part):
+        to = lax.rem(z + dist, n_sp)
+        return remote(
+            zsend.at[to, c, spans[part]],
+            zrecv.at[z, c, spans[part]],
+            zs_sem.at[dist, c, part],
+            zr_sem.at[dist, c, part],
+            {"sp": to},
+        )
+
+    def z_arrival(dist, c, part):
+        src = lax.rem(z + n_sp - dist, n_sp)
+        return remote(
+            zsend.at[src, c, spans[part]],
+            zrecv.at[src, c, spans[part]],
+            zs_sem.at[dist, c, part],
+            zr_sem.at[dist, c, part],
+            {"sp": src},
+        )
 
     def finish_chunk(c):
         r = pl.ds(c * rc, rc)
@@ -383,13 +406,18 @@
         total = total * rms
         for h in range(heads):
             zsend[h, c, :rc] = total[:, 2 * h * hd : 2 * (h + 1) * hd].astype(bf16)
-            v_h = total[:, 2 * attn_w + h * hd : 2 * attn_w + (h + 1) * hd]
-            zsend[h, c, rc:] = jnp.concatenate([v_h[:half], v_h[half:]], axis=1).astype(bf16)
+            q_h = total[:, 2 * attn_w + h * hd : 2 * attn_w + (h + 1) * hd]
+            zsend[h, c, rc:] = jnp.concatenate([q_h[:half], q_h[half:]], axis=1).astype(bf16)
         for dist in range(n_sp - 1, 0, -1):
-            to = lax.rem(z + dist, n_sp)
-            remote(
-                zsend.at[to, c], zrecv.at[z, c], zs_sem.at[dist, c], zr_sem.at[dist, c], {"sp": to}
-            ).start()
+
+            @pl.when(z < n_sp - 1)
+            def _():
+                z_copy(dist, c, 0).start()
+
+            @pl.when(z > 0)
+            def _():
+                z_copy(dist, c, 1).start()
+
         zrecv[z, c] = zsend[z, c]
 
     rim = halo.shape[0]
@@ -476,46 +504,75 @@
         )
         cp.start()
         stats.append(cp)
-    for dist in range(n_sp - 1, 0, -1):
-        for c in range(AG_CHUNKS):
-            src = lax.rem(z + dist, n_sp)
-            remote(
-                zsend.at[src, c],
-                zrecv.at[src, c],
-                zs_sem.at[n_sp - dist, c],
-                zr_sem.at[n_sp - dist, c],
-                {"sp": src},
-            ).wait_recv()
     scale = hd ** (-0.5)
-    low = lax.broadcasted_iota(jnp.int32, (half, 2 * hd), 1) < hd
-    for s in range(n_sp):
-        for c in range(AG_CHUNKS):
-            r0 = s * rows + c * rc
-            tile = zrecv[s, c, :rc].astype(f32)
-            q_s[pl.ds(r0, rc)] = (tile[:, :hd] * scale).astype(bf16)
-            k_s[pl.ds(r0, rc)] = tile[:, hd:].astype(bf16)
-            vt = zrecv[s, c, rc:].astype(f32)
-            v_s[pl.ds(r0, half)] = jnp.where(low, vt, 1.0).astype(bf16)
-            v_s[pl.ds(r0 + half, half)] = jnp.where(low, pltpu.roll(vt, hd, 1), 1.0).astype(bf16)
-    v_t[...] = v_s[...].T
+    low = lax.broadcasted_iota(jnp.int32, (rc, 2 * hd), 1) < hd
     wide_k = -(-rows // 128)
     allowed = lax.broadcasted_iota(jnp.int32, (rows, rows), 0) <= lax.broadcasted_iota(
         jnp.int32, (rows, rows), 1
     )
-    for i in [k // 2 if k % 2 == 0 else n_sp - 1 - k // 2 for k in range(n_sp)]:
-        keys = (i + 1) * rows
-        q = q_s[pl.ds(i * rows, rows)]
-        cum_k = jnp.concatenate([cum_col[:keys]] * wide_k, axis=1)
-        sc = lax.dot_general(k_s[:keys], q, NT, preferred_element_type=f32) - cum_k
-        diag = jnp.where(allowed, sc[keys - rows :], -jnp.inf)
-        sc = diag if i == 0 else jnp.concatenate([sc[: keys - rows], diag], axis=0)
+
+    def take_keys(tile, r0):
+        kv = tile.astype(f32)
+        k_s[pl.ds(r0, rc)] = kv[:, :hd].astype(bf16)
+        v_s[pl.ds(r0, rc)] = jnp.where(low, pltpu.roll(kv, hd, 1), 1.0).astype(bf16)
+
+    def take_queries(tile, r0):
+        qt = tile.astype(f32) * scale
+        q_s[pl.ds(r0, half)] = qt[:, :hd].astype(bf16)
+        q_s[pl.ds(r0 + half, half)] = qt[:, hd:].astype(bf16)
+
+    def attend(q, k, vt, cum_k, causal):
+        sc = lax.dot_general(k, q, NT, preferred_element_type=f32) - cum_k
+        if causal:
+            sc = jnp.where(allowed, sc, -jnp.inf)
         top = jnp.max(sc, axis=0, keepdims=True)
         p = jnp.exp(sc - top).astype(bf16)
-        both = jnp.dot(v_t[:, :keys], p, preferred_element_type=f32)
+        both = jnp.dot(vt, p, preferred_element_type=f32)
         tot = both[hd : hd + 1]
-        ret_send[i] = (both[:hd] / tot).astype(bf16)
-        lse = top + jnp.log(tot) + cum_recv[i, pl.ds(z, 1)]
-        lse_send[i] = jnp.broadcast_to(lse, (8, rows))
+        return both[:hd] / tot, top + jnp.log(tot)
+
+    for h in range(heads):
+        for c in range(AG_CHUNKS):
+            take_keys(zsend[h, c, :rc], h * rows + c * rc)
+            take_queries(zsend[h, c, rc:], h * rows + c * rc)
+    v_t[...] = v_s[...].T
+    for h in range(heads):
+        own = pl.ds(h * rows, rows)
+        own_cum = cum_ref[pl.ds(h, 1), :]
+        col = jnp.broadcast_to(own_cum, (128, rows)).T
+        out_loc[pl.ds(h * hd, hd), :], lse = attend(
+            q_s[own], k_s[own], v_t[:, h * rows : (h + 1) * rows],
+            jnp.concatenate([col] * wide_k, axis=1), True,
+        )
+        lse_loc[pl.ds(h, 1), :] = lse + own_cum
+    for dist in range(1, n_sp):
+        src = lax.rem(z + n_sp - dist, n_sp)
+        for c in range(AG_CHUNKS):
+
+            @pl.when(src < n_sp - 1)
+            def _():
+                z_arrival(dist, c, 0).wait_recv()
+
+            @pl.when(src > 0)
+            def _():
+                z_arrival(dist, c, 1).wait_recv()
+
+    for s in range(n_sp):
+        for c in range(AG_CHUNKS):
+            if s < n_sp - 1:
+                take_keys(zrecv[s, c, :rc], s * rows + c * rc)
+            if s > 0:
+                take_queries(zrecv[s, c, rc:], s * rows + c * rc)
+    far_keys = (n_sp - 1) * rows
+    v_t[:, :far_keys] = v_s[:far_keys].T
+    for i in [1 + k // 2 if k % 2 == 0 else n_sp - 1 - k // 2 for k in range(n_sp - 1)]:
+        keys = i * rows
+        o, lse = attend(
+            q_s[pl.ds(i * rows, rows)], k_s[:keys], v_t[:, :keys],
+            jnp.concatenate([cum_col[:keys]] * wide_k, axis=1), False,
+        )
+        ret_send[i] = o.astype(bf16)
+        lse_send[i] = jnp.broadcast_to(lse + cum_recv[i, pl.ds(z, 1)], (8, rows))
 
         @pl.when(z != i)
         def _():
@@ -545,7 +602,7 @@
 
     for h in range(n_sp):
 
-        @pl.when(z != h)
+        @pl.when((z != h) & (z > 0))
         def _():
             remote(
                 ret_send.at[h], ret_recv.at[h], rs_sem.at[h], rr_sem.at[h], {"sp": h}
@@ -554,9 +611,22 @@
                 lse_send.at[h], lse_recv.at[h], ls_sem.at[h], lr_sem.at[h], {"sp": h}
             ).wait_recv()
 
-    att_s[...] = jnp.concatenate([ret_recv[h] for h in range(n_sp)], axis=0).astype(f32).T.astype(bf16)
-    for h in range(n_sp):
-        log_ref[pl.ds(h, 1), :] = lse_recv[h, 0:1, :]
+    @pl.when(z == 0)
+    def _():
+        log_ref[...] = lse_loc[...]
+
+    @pl.when(z > 0)
+    def _():
+        for h in range(heads):
+            r = pl.ds(h * hd, hd)
+            near, far = lse_loc[pl.ds(h, 1), :], lse_recv[h, 0:1, :]
+            top = jnp.maximum(near, far)
+            w_near, w_far = jnp.exp(near - top), jnp.exp(far - top)
+            tot = w_near + w_far
+            out_loc[r, :] = (out_loc[r, :] * w_near + ret_recv[h].astype(f32) * w_far) / tot
+            log_ref[pl.ds(h, 1), :] = top + jnp.log(tot)
+
+    att_s[...] = out_loc[...].T.astype(bf16)
     wao_copy.wait()
     own_rows = rows // n_tp
     cw = d_all // OUT_CHUNKS
@@ -619,12 +689,17 @@
         halo_copy.wait_send()
 
     for dist in range(1, n_sp):
-        to = lax.rem(z + dist, n_sp)
         for c in range(AG_CHUNKS):
-            remote(
-                zsend.at[to, c], zrecv.at[z, c], zs_sem.at[dist, c], zr_sem.at[dist, c], {"sp": to}
-            ).wait_send()
-    for i in range(n_sp):
+
+            @pl.when(z < n_sp - 1)
+            def _():
+                z_copy(dist, c, 0).wait_send()
+
+            @pl.when(z > 0)
+            def _():
+                z_copy(dist, c, 1).wait_send()
+
+    for i in range(1, n_sp):
 
         @pl.when(z != i)
         def _():
@@ -679,6 +754,8 @@
         pltpu.VMEM((n_sp * rows, hd), bf16),
         pltpu.VMEM((n_sp * rows, 2 * hd), bf16),
         pltpu.VMEM((2 * hd, n_sp * rows), bf16),
+        pltpu.VMEM((attn_w, rows), f32),
+        pltpu.VMEM((heads, rows), f32),
         pltpu.VMEM((n_sp * rows, 128), f32),
         pltpu.VMEM((n_sp, heads, rows), f32),
         pltpu.VMEM((rows + rim, conv_w), f32),
@@ -703,8 +780,8 @@
         dma,
         dma((n_tp, AG_CHUNKS)),
         dma((n_tp, AG_CHUNKS)),
-        dma((n_sp, AG_CHUNKS)),
-        dma((n_sp, AG_CHUNKS)),
+        dma((n_sp, AG_CHUNKS, 2)),
+        dma((n_sp, AG_CHUNKS, 2)),
         dma((n_sp,)),
         dma((n_sp,)),
         dma,

time: 39.8 us -> 38.4 us (0.965)
  the two profiles are of different devices: /device:TPU:0 before, /device:TPU:17 now
where the time goes in v4:
time: 38.4 us; the launch traced here: 38.1 us
  Pallas kernels  36.1 us (94%)
  local copies, waits for them, and re-layouts  1.3 us (3%)
  between operations  0.64 us (2%)
    pallas_call x1, Pallas kernels, fused_local(): pl.pallas_call(functools.partial(fused_kernel, n_sp, n_tp), out_shape=(pl...  36.1 us
    unnamed x2, local copies, waits for them, and re-layouts  1.3 us

profile of v4, /device:TPU:17, one launch (start us, length us, event | category | flops | bytes accessed | tf_op | source)
XLA Modules:
  0.0 38.1 jit_solution(12778454906286370870)
XLA Ops:
  0.6 36.1 %shard_map.131 = (bf16[64,2048]{1,0:T(8,128)(2,1)S(1)}, f32[4,256]{1,0:T(4,128)S(1)}) custom-call(bf16[256,512]{1,0:T(8,128)(2,1)} %x_hbm.1, bf16[2048]{0:T(1024)(128)(2,1)} %gain_ref.1, bf16[256,2048]{1,0:T(8,128)(2,1)} %wci_hbm.1, bf16[256,2048]{1,0:T(8,128)(2,1)} %wcg_hbm.1, bf16[31,256]{1,0:T(8,128)(2,1)} %ck_ref.1, bf16[256]{0:T(256)(128)(2,1)} %lng_ref.1, ...), custom_call_target="tpu_custom_call" | custom-call | tf_op jit(solution)/shard_map/pallas_call | solution.py:802
  36.8 0.7 %copy.16 = bf16[64,2048]{1,0:T(8,128)(2,1)} copy(bf16[64,2048]{1,0:T(8,128)(2,1)S(1)} %get-tuple-element.2) | data formatting | bytes 524288
  37.5 0.6 %copy.17 = f32[4,256]{1,0:T(4,128)} copy(f32[4,256]{1,0:T(4,128)S(1)} %get-tuple-element.3) | data formatting | bytes 8192

commit v5 on v4

--- a/solution.py
+++ b/solution.py
@@ -162,7 +162,7 @@
     return (mixed, log_total)
 
 
-AG_CHUNKS = 8
+AG_CHUNKS = 4
 OUT_CHUNKS = 4
 MESH = pl.DeviceIdType.MESH
 NT = (((1,), (1,)), ((), ()))

time: 38.4 us -> 35.8 us (0.932)
  the two profiles are of different devices: /device:TPU:17 before, /device:TPU:11 now
where the time goes in v5:
time: 35.8 us; the launch traced here: 35.5 us
  Pallas kernels  33.5 us (94%)
  local copies, waits for them, and re-layouts  1.3 us (4%)
  between operations  0.64 us (2%)
    pallas_call x1, Pallas kernels, fused_local(): pl.pallas_call(functools.partial(fused_kernel, n_sp, n_tp), out_shape=(pl...  33.5 us
    unnamed x2, local copies, waits for them, and re-layouts  1.3 us

profile of v5, /device:TPU:11, one launch (start us, length us, event | category | flops | bytes accessed | tf_op | source)
XLA Modules:
  0.0 35.5 jit_solution(15091003941161989857)
XLA Ops:
  0.6 33.5 %shard_map.131 = (bf16[64,2048]{1,0:T(8,128)(2,1)S(1)}, f32[4,256]{1,0:T(4,128)S(1)}) custom-call(bf16[256,512]{1,0:T(8,128)(2,1)} %x_hbm.1, bf16[2048]{0:T(1024)(128)(2,1)} %gain_ref.1, bf16[256,2048]{1,0:T(8,128)(2,1)} %wci_hbm.1, bf16[256,2048]{1,0:T(8,128)(2,1)} %wcg_hbm.1, bf16[31,256]{1,0:T(8,128)(2,1)} %ck_ref.1, bf16[256]{0:T(256)(128)(2,1)} %lng_ref.1, ...), custom_call_target="tpu_custom_call" | custom-call | tf_op jit(solution)/shard_map/pallas_call | solution.py:802
  34.2 0.7 %copy.16 = bf16[64,2048]{1,0:T(8,128)(2,1)} copy(bf16[64,2048]{1,0:T(8,128)(2,1)S(1)} %get-tuple-element.2) | data formatting | bytes 524288
  34.9 0.6 %copy.17 = f32[4,256]{1,0:T(4,128)} copy(f32[4,256]{1,0:T(4,128)S(1)} %get-tuple-element.3) | data formatting | bytes 8192
